TPU v7x, 32 devices: a whole 2x2x4 slice. The times are simulated.
32 devices in a mesh: sp: 4 (over z), fs: 4 (over y, x), tp: 2 (over core).
Axes of the slice: x: 2, y: 2, z: 4, core: 2. Of those that a mesh axis runs over, the one named last changes fastest.
Arguments:
- stream: bfloat16 [4, 1024, 4096], P('fs', 'sp'), may hold values from -6 to 6
- norm_gain: float32 [4096], replicated, may hold values from 0.1 to 1.9
- value_proj: bfloat16 [4096, 1024], P(('sp', 'fs'), 'tp'), may hold values from -0.09375 to 0.09375
- gate_proj: bfloat16 [4096, 1024], P(('sp', 'fs'), 'tp'), may hold values from -0.09375 to 0.09375
- state_proj: bfloat16 [4096, 1024], P(('sp', 'fs'), 'tp'), may hold values from -0.09375 to 0.09375
- conv_kernel: bfloat16 [31, 1024], P(None, 'tp'), may hold values from -1 to 1
- conv_gain: float32 [1024], P('tp'), may hold values from 0.1 to 1.9
- decay_rate: float32 [64, 64], P('tp'), may hold values from 0.25 to 1
- frequency: float32 [64, 64], P('tp'), may hold values from 0 to 201.06177
- log_step: float32 [64], P('tp'), may hold values from -12 to -2.3
- step_gain: float32 [4, 64, 1024], P('fs', 'tp', 'sp'), may hold values from 0.35 to 614.4
- drive_matrix: float32 [2, 64, 64, 16], P(None, 'tp'), may hold values from -1 to 1
- read_matrix: float32 [2, 64, 16, 64], P(None, 'tp'), may hold values from -0.5 to 0.5
- skip_gain: float32 [1024], P('tp'), may hold values from -4 to 4
- start_state: float32 [2, 4, 64, 64], P(None, 'fs', 'tp'), may hold values from -6 to 6
- merge_conv: bfloat16 [4096, 1024], P(('sp', 'fs'), 'tp'), may hold values from -0.125 to 0.125
- merge_state: bfloat16 [4096, 1024], P(('sp', 'fs'), 'tp'), may hold values from -0.125 to 0.125
Outputs:
- mixed: bfloat16 [4, 1024, 4096], P('fs', ('sp', 'tp'))
All inputs are finite; a program needn't handle non-finite values.
Results may differ from a plain program's by a relative error of at most 0.014.
Values may be sent and summed in bfloat16 or wider, within the bound.
A program may use at most 256 MiB of HBM per device.

v0:
```python
import jax
import jax.numpy as jnp
from jax import lax
from jax.sharding import PartitionSpec as P

HEAD_CH = 128


exact_mode = lax.Precision.HIGHEST


def shifted(value, axis, steps):
    count = lax.axis_size(axis)
    initial, last = (max(0, -steps), min(count, count - steps))
    return lax.ppermute(value, axis, [(source, source + steps) for source in range(initial, last)])


def carried_in(part, axis, combine, identity):
    place = lax.axis_index(axis)
    gathered = jax.tree.map(lambda a: lax.all_gather(a, axis), part)
    state = jax.tree.map(lambda a, e: jnp.zeros_like(a) + jnp.asarray(e, a.dtype), part, identity)

    def one(hop, state):
        return combine(
            state, jax.tree.map(lambda a: lax.dynamic_index_in_dim(a, hop, 0, False), gathered)
        )

    return lax.fori_loop(0, place, one, state)


def link_states(earlier, later):
    return (
        later[0] * earlier[0] - later[1] * earlier[1],
        later[0] * earlier[1] + later[1] * earlier[0],
        later[0] * earlier[2] - later[1] * earlier[3] + later[2],
        later[0] * earlier[3] + later[1] * earlier[2] + later[3],
    )


def body(
    stream,
    norm_gain,
    value_proj,
    gate_proj,
    state_proj,
    conv_kernel,
    conv_gain,
    decay_rate,
    frequency,
    log_step,
    step_gain,
    drive_matrix,
    read_matrix,
    skip_gain,
    start_state,
    merge_conv,
    merge_state,
):
    row_count = stream.shape[1]
    gathered = (
        lax.all_gather(value_proj, ("sp", "fs"), axis=0, tiled=True),
        lax.all_gather(gate_proj, ("sp", "fs"), axis=0, tiled=True),
        lax.all_gather(state_proj, ("sp", "fs"), axis=0, tiled=True),
        lax.all_gather(merge_conv, ("sp", "fs"), axis=0, tiled=True),
        lax.all_gather(merge_state, ("sp", "fs"), axis=0, tiled=True),
    )
    value_whole, gate_whole, state_whole, conv_merge, state_merge = gathered
    widened = stream[0].astype(jnp.float32)
    inverse = lax.rsqrt(jnp.mean(widened * widened, axis=1, keepdims=True) + 1e-06)
    normed = (widened * inverse * norm_gain).astype(jnp.bfloat16)
    value_pre = jnp.dot(normed, value_whole, preferred_element_type=jnp.float32)
    gate_pre = jnp.dot(normed, gate_whole, preferred_element_type=jnp.float32)
    gated = (value_pre * jax.nn.sigmoid(gate_pre)).astype(jnp.bfloat16)
    scan_input = jnp.dot(normed, state_whole, preferred_element_type=jnp.float32).astype(
        jnp.bfloat16
    )
    group_count, state_size = decay_rate.shape
    group_width = drive_matrix.shape[3]
    flat_width = group_count * state_size
    inputs_flat = scan_input.astype(jnp.float32)
    inputs_rows = inputs_flat.reshape(row_count, group_count, group_width)
    drive_re = jnp.einsum("gnc,rgc->rgn", drive_matrix[0], inputs_rows, precision=exact_mode)
    drive_im = jnp.einsum("gnc,rgc->rgn", drive_matrix[1], inputs_rows, precision=exact_mode)
    step_size = jnp.transpose(jnp.exp(log_step)[:, None] * step_gain[0])[:, :, None]
    rate_row = decay_rate[None]
    turn_row = frequency[None]
    modulus = jnp.exp(-step_size * rate_row)
    rotation = step_size * turn_row
    trans_re = modulus * jnp.cos(rotation)
    trans_im = modulus * jnp.sin(rotation)
    magnitude = rate_row * rate_row + turn_row * turn_row
    less_re = trans_re - 1.0
    factor_re = (-rate_row * less_re + turn_row * trans_im) / magnitude
    factor_im = (-rate_row * trans_im - turn_row * less_re) / magnitude
    push_re = factor_re * drive_re - factor_im * drive_im
    push_im = factor_re * drive_im + factor_im * drive_re
    running = lax.associative_scan(
        link_states,
        (
            trans_re.reshape(row_count, flat_width),
            trans_im.reshape(row_count, flat_width),
            push_re.reshape(row_count, flat_width),
            push_im.reshape(row_count, flat_width),
        ),
        axis=0,
    )
    unit_part = jnp.ones((group_count, state_size), jnp.float32)
    zero_part = jnp.zeros((group_count, state_size), jnp.float32)
    last_re = running[0][-1].reshape(group_count, state_size)
    last_im = running[1][-1].reshape(group_count, state_size)
    last_sre = running[2][-1].reshape(group_count, state_size)
    last_sim = running[3][-1].reshape(group_count, state_size)
    margin = conv_kernel.shape[0] - 1
    edge_rows = gated[row_count - margin :]
    before = shifted(edge_rows, "sp", 1)
    prefix = carried_in(
        (last_re, last_im, last_sre, last_sim),
        "sp",
        link_states,
        (unit_part, zero_part, zero_part, zero_part),
    )
    init_re = start_state[0, 0]
    init_im = start_state[1, 0]
    enter_re = (prefix[0] * init_re - prefix[1] * init_im + prefix[2]).reshape(1, flat_width)
    enter_im = (prefix[0] * init_im + prefix[1] * init_re + prefix[3]).reshape(1, flat_width)
    state_re = running[2] + running[0] * enter_re - running[1] * enter_im
    state_im = running[3] + running[0] * enter_im + running[1] * enter_re
    state_re = state_re.reshape(row_count, group_count, state_size)
    state_im = state_im.reshape(row_count, group_count, state_size)
    read_out = jnp.einsum(
        "gcn,rgn->rgc", read_matrix[0], state_re, precision=exact_mode
    ) - jnp.einsum("gcn,rgn->rgc", read_matrix[1], state_im, precision=exact_mode)
    read_out = read_out.reshape(row_count, group_count * group_width)
    state_out = jax.nn.gelu(read_out + skip_gain * inputs_flat).astype(jnp.bfloat16)
    padded = jnp.concatenate([before, gated], axis=0).astype(jnp.float32)
    kernel = conv_kernel.astype(jnp.float32)
    mixed_taps = kernel[0] * padded[0:row_count]
    for tap_index in range(1, margin + 1):
        mixed_taps = mixed_taps + kernel[tap_index] * padded[tap_index : tap_index + row_count]
    grouped = mixed_taps.reshape(row_count, -1, HEAD_CH)
    center = grouped - jnp.mean(grouped, axis=2, keepdims=True)
    spread = jnp.mean(center * center, axis=2, keepdims=True)
    normal = (center * lax.rsqrt(spread + 1e-05)).reshape(row_count, -1) * conv_gain
    conv_out = (normal * jax.nn.sigmoid(normal)).astype(jnp.bfloat16)
    conv_term = lax.dot_general(
        conv_out, conv_merge, (((1,), (1,)), ((), ())), preferred_element_type=jnp.float32
    )
    state_term = lax.dot_general(
        state_out, state_merge, (((1,), (1,)), ((), ())), preferred_element_type=jnp.float32
    )
    mixed = lax.psum_scatter(
        (conv_term + state_term).astype(jnp.bfloat16), "tp", scatter_dimension=0, tiled=True
    )
    return mixed[None]


def solution(mesh):
    return jax.shard_map(
        body,
        mesh=mesh,
        in_specs=(
            P("fs", "sp", None),
            P(),
            P(("sp", "fs"), "tp"),
            P(("sp", "fs"), "tp"),
            P(("sp", "fs"), "tp"),
            P(None, "tp"),
            P("tp"),
            P("tp", None),
            P("tp", None),
            P("tp"),
            P("fs", "tp", "sp"),
            P(None, "tp", None, None),
            P(None, "tp", None, None),
            P("tp"),
            P(None, "fs", "tp", None),
            P(("sp", "fs"), "tp"),
            P(("sp", "fs"), "tp"),
        ),
        out_specs=P("fs", ("sp", "tp"), None),
        check_vma=False,
    )
```

profile of v0, /device:TPU:0, one launch (start us, length us, event | category | flops | bytes accessed | tf_op | source)
XLA Modules:
  0.0 2356.0 jit_solution(1497417654694736751)
XLA Ops:
  23.7 39.8 %slice.759 = f32[128,2048]{0,1:T(8,128)} slice(f32[256,2048]{0,1:T(8,128)} %get-tuple-element.222), slice={[1:256:2], [0:2048:1]} | slice | bytes 2097152 | tf_op jit(solution)/shard_map/slice | solution.py:97
  63.5 39.8 %slice.765 = f32[128,2048]{0,1:T(8,128)} slice(f32[256,2048]{0,1:T(8,128)} %get-tuple-element.222), slice={[0:255:2], [0:2048:1]} | slice | bytes 2097152 | tf_op jit(solution)/shard_map/slice | solution.py:97
  103.2 39.2 %slice.761 = f32[128,2048]{0,1:T(8,128)} slice(f32[256,2048]{0,1:T(8,128)S(1)} %get-tuple-element.223), slice={[1:256:2], [0:2048:1]} | slice | bytes 2097152 | tf_op jit(solution)/shard_map/slice | solution.py:97
  142.4 39.4 %slice.766 = f32[128,2048]{0,1:T(8,128)} slice(f32[256,2048]{0,1:T(8,128)S(1)} %get-tuple-element.223), slice={[0:255:2], [0:2048:1]} | slice | bytes 2097152 | tf_op jit(solution)/shard_map/slice | solution.py:97
  181.8 39.5 %slice.758 = f32[127,2048]{0,1:T(8,128)} slice(f32[256,2048]{0,1:T(8,128)} %get-tuple-element.222), slice={[2:256:2], [0:2048:1]} | slice | bytes 2080768 | tf_op jit(solution)/shard_map/slice | solution.py:97
  221.3 38.9 %slice.868 = f32[127,2048]{0,1:T(8,128)} slice(f32[256,2048]{0,1:T(8,128)S(1)} %get-tuple-element.223), slice={[2:256:2], [0:2048:1]} | slice | bytes 2080768 | tf_op jit(solution)/shard_map/slice | solution.py:97
  283.1 39.2 %slice.760 = f32[128,2048]{0,1:T(8,128)} slice(f32[256,2048]{0,1:T(8,128)S(1)} %bitcast.239), slice={[0:255:2], [0:2048:1]} | slice | bytes 2097152 | tf_op jit(solution)/shard_map/slice | solution.py:97
  322.2 39.2 %slice.763 = f32[128,2048]{0,1:T(8,128)} slice(f32[256,2048]{0,1:T(8,128)S(1)} %bitcast.240), slice={[1:256:2], [0:2048:1]} | slice | bytes 2097152 | tf_op jit(solution)/shard_map/slice | solution.py:97
  361.4 39.9 %slice.762 = f32[128,2048]{0,1:T(8,128)} slice(f32[256,2048]{0,1:T(8,128)} %bitcast.242), slice={[0:255:2], [0:2048:1]} | slice | bytes 2097152 | tf_op jit(solution)/shard_map/slice | solution.py:97
  401.3 39.2 %slice.771 = f32[128,2048]{0,1:T(8,128)} slice(f32[256,2048]{0,1:T(8,128)S(1)} %bitcast.244), slice={[1:256:2], [0:2048:1]} | slice | bytes 2097152 | tf_op jit(solution)/shard_map/slice | solution.py:97
  465.9 21.9 slice.773
  487.8 21.9 slice.768
  530.0 21.9 slice.770
  592.5 22.1 slice.781
  1053.2 21.6 slice.767
  1074.9 21.6 slice.862
  1096.5 22.0 slice.866
  1139.4 39.5 %slice.872 = f32[127,2048]{0,1:T(8,128)} slice(f32[256,2048]{0,1:T(8,128)} %bitcast.241), slice={[2:256:2], [0:2048:1]} | slice | bytes 2080768 | tf_op jit(solution)/shard_map/slice | solution.py:97
  1178.9 39.5 %slice.910 = f32[127,2048]{0,1:T(8,128)} slice(f32[256,2048]{0,1:T(8,128)} %bitcast.243), slice={[2:256:2], [0:2048:1]} | slice | bytes 2080768 | tf_op jit(solution)/shard_map/slice | solution.py:97
  1712.6 22.0 pad.222
  1734.6 22.4 pad.223
  1759.7 43.6 %pad.259 = f32[256,2048]{0,1:T(8,128)} pad(f32[128,2048]{0,1:T(8,128)} %add.688, f32[]{:T(128)} %constant.17.clone.1), padding=1_0_1x0_0_0 | pad | bytes 3145732 | tf_op jit(solution)/shard_map/pad | solution.py:97
  1825.3 22.5 pad.221
  1854.6 39.3 %pad.258 = f32[256,2048]{0,1:T(8,128)} pad(f32[128,2048]{0,1:T(8,128)S(1)} %pad_maximum_fusion.15, f32[]{:T(128)} %constant.17.clone.1), padding=0_1_1x0_0_0 | pad | bytes 3145732 | tf_op jit(solution)/shard_map/pad | solution.py:97
  1896.5 43.6 %pad.225 = f32[256,2048]{0,1:T(8,128)} pad(f32[128,2048]{0,1:T(8,128)} %add.685, f32[]{:T(128)} %constant.17.clone.1), padding=1_0_1x0_0_0 | pad | bytes 3145732 | tf_op jit(solution)/shard_map/pad | solution.py:97
  1942.6 43.4 %pad.224 = f32[256,2048]{0,1:T(8,128)} pad(f32[128,2048]{0,1:T(8,128)} %pad_maximum_fusion.6, f32[]{:T(128)} %constant.17.clone.1), padding=0_1_1x0_0_0 | pad | bytes 3145732 | tf_op jit(solution)/shard_map/pad | solution.py:97
  2029.7 22.5 pad.251
  2054.7 22.0 pad.250
  2083.2 39.1 %pad.256 = f32[256,2048]{0,1:T(8,128)S(1)} pad(f32[128,2048]{0,1:T(8,128)} %pad_maximum_fusion.14, f32[]{:T(128)} %constant.17.clone.1), padding=0_1_1x0_0_0 | pad | bytes 3145732 | tf_op jit(solution)/shard_map/pad | solution.py:97
  2122.3 39.8 %pad.257 = f32[256,2048]{0,1:T(8,128)} pad(f32[128,2048]{0,1:T(8,128)S(1)} %copy-done.119, f32[]{:T(128)} %constant.17.clone.1), padding=1_0_1x0_0_0 | pad | bytes 3145732 | tf_op jit(solution)/shard_map/pad | solution.py:97
  2167.1 39.2 %pad.254 = f32[256,2048]{0,1:T(8,128)S(1)} pad(f32[128,2048]{0,1:T(8,128)} %pad_maximum_fusion.13, f32[]{:T(128)} %constant.17.clone.1), padding=0_1_1x0_0_0 | pad | bytes 3145732 | tf_op jit(solution)/shard_map/pad | solution.py:97
  2206.4 39.6 %pad.255 = f32[256,2048]{0,1:T(8,128)} pad(f32[128,2048]{0,1:T(8,128)S(1)} %copy-done.113, f32[]{:T(128)} %constant.17.clone.1), padding=1_0_1x0_0_0 | pad | bytes 3145732 | tf_op jit(solution)/shard_map/pad | solution.py:97
  (659 shorter events, 1275.5 us)
Async XLA Ops:
  6.5 257.1 %all-gather.12.cloned.1.call-start = ((), (), s32[]{:S(2)}) async-start(), calls=%async_computation.4 | async-start | bytes 4456448 | tf_op jit(solution)/shard_map/all_gather | solution.py:63
  7.3 2295.4 %all-gather.8.cloned.1.call-start = ((), (), s32[]{:S(2)}) async-start(), calls=%async_computation.2 | async-start | bytes 4456448 | tf_op jit(solution)/shard_map/all_gather | solution.py:62
  8.0 2298.9 %all-gather.6.cloned.1.call-start = ((), (), s32[]{:S(2)}) async-start(), calls=%async_computation.1 | async-start | bytes 4456448 | tf_op jit(solution)/shard_map/all_gather | solution.py:61
  8.7 2317.4 %all-gather.10.cloned.1.call-start = ((), (), s32[]{:S(2)}) async-start(), calls=%async_computation.3 | async-start | bytes 4456448 | tf_op jit(solution)/shard_map/all_gather | solution.py:64
  9.3 2323.1 %all-gather.14.cloned.1.call-start = ((), (), s32[]{:S(2)}) async-start(), calls=%async_computation.5 | async-start | bytes 4456448 | tf_op jit(solution)/shard_map/all_gather | solution.py:65
  9.9 2338.8 %reduce-scatter.2.cloned.1.call-start = ((), (), s32[]{:S(2)}) async-start(), calls=%async_computation.6 | async-start | bytes 3145728 | tf_op jit(solution)/shard_map/reduce_scatter | solution.py:151
  181.8 78.4 %copy-start.128 = (bf16[31,512]{1,0:T(8,128)(2,1)S(1)}, bf16[31,512]{1,0:T(8,128)(2,1)}, u32[]{:S(2)}) copy-start(bf16[31,512]{1,0:T(8,128)(2,1)} %param.24) | copy-start | bytes 95236
  221.3 42.9 %copy-start.167 = (f32[4096]{0:T(1024)S(1)}, f32[4096]{0:T(1024)}, u32[]{:S(2)}) copy-start(f32[4096]{0:T(1024)} %param.20) | copy-start | bytes 49156
  283.0 78.4 %copy-start.98 = (f32[256,32,64]{0,2,1:T(8,128)}, f32[256,32,64]{0,2,1:T(8,128)S(1)}, u32[]{:S(2)}) copy-start(f32[256,32,64]{0,2,1:T(8,128)S(1)} %get-tuple-element.112) | copy-start | bytes 6291460
  361.4 39.9 %copy-start.100 = (f32[256,32,64]{0,2,1:T(8,128)S(1)}, f32[256,32,64]{0,2,1:T(8,128)}, u32[]{:S(2)}) copy-start(f32[256,32,64]{0,2,1:T(8,128)} %get-tuple-element.111) | copy-start | bytes 6291460
  445.4 42.4 %copy-start.2 = (f32[128,2048]{0,1:T(8,128)}, f32[128,2048]{0,1:T(8,128)S(1)}, u32[]{:S(2)}) copy-start(f32[128,2048]{0,1:T(8,128)S(1)} %get-tuple-element.211) | copy-start | bytes 3145732
  445.4 106.5 %copy-start = (f32[128,2048]{0,1:T(8,128)}, f32[128,2048]{0,1:T(8,128)S(1)}, u32[]{:S(2)}) copy-start(f32[128,2048]{0,1:T(8,128)S(1)} %get-tuple-element.140) | copy-start | bytes 3145732
  530.0 42.2 %copy-start.4 = (f32[128,2048]{0,1:T(8,128)S(1)}, f32[128,2048]{0,1:T(8,128)}, u32[]{:S(2)}) copy-start(f32[128,2048]{0,1:T(8,128)} %get-tuple-element.212) | copy-start | bytes 3145732
  619.9 34.4 %copy-start.6 = (f32[64,2048]{0,1:T(8,128)}, f32[64,2048]{0,1:T(8,128)S(1)}, u32[]{:S(2)}) copy-start(f32[64,2048]{0,1:T(8,128)S(1)} %get-tuple-element.210) | copy-start | bytes 1572868
  619.9 56.4 %copy-start.8 = (f32[64,2048]{0,1:T(8,128)}, f32[64,2048]{0,1:T(8,128)S(1)}, u32[]{:S(2)}) copy-start(f32[64,2048]{0,1:T(8,128)S(1)} %get-tuple-element.209) | copy-start | bytes 1572868
  665.1 22.0 copy-start.12
  714.4 23.6 %copy-start.15 = (f32[32,2048]{0,1:T(8,128)}, f32[32,2048]{0,1:T(8,128)S(1)}, u32[]{:S(2)}) copy-start(f32[32,2048]{0,1:T(8,128)S(1)} %get-tuple-element.131) | copy-start | bytes 786436
  714.4 36.6 %copy-start.17 = (f32[32,2048]{0,1:T(8,128)}, f32[32,2048]{0,1:T(8,128)S(1)}, u32[]{:S(2)}) copy-start(f32[32,2048]{0,1:T(8,128)S(1)} %get-tuple-element.132) | copy-start | bytes 786436
  776.0 29.8 %copy-start.24 = (f32[16,2048]{0,1:T(8,128)}, f32[16,2048]{0,1:T(8,128)S(1)}, u32[]{:S(2)}) copy-start(f32[16,2048]{0,1:T(8,128)S(1)} %get-tuple-element.206) | copy-start | bytes 393220
  826.1 31.2 %copy-start.28 = (f32[8,2048]{0,1:T(8,128)}, f32[8,2048]{0,1:T(8,128)S(1)}, u32[]{:S(2)}) copy-start(f32[8,2048]{0,1:T(8,128)S(1)} %get-tuple-element.124) | copy-start | bytes 196612
  826.1 39.7 %copy-start.27 = (f32[8,2048]{0,1:T(8,128)}, f32[8,2048]{0,1:T(8,128)S(1)}, u32[]{:S(2)}) copy-start(f32[8,2048]{0,1:T(8,128)S(1)} %get-tuple-element.204) | copy-start | bytes 196612
  1042.4 32.4 %copy-start.1 = (f32[128,2048]{0,1:T(8,128)S(1)}, f32[128,2048]{0,1:T(8,128)}, u32[]{:S(2)}) copy-start(f32[128,2048]{0,1:T(8,128)} %copy-done) | copy-start | bytes 3145732
  1053.2 43.2 %copy-start.3 = (f32[128,2048]{0,1:T(8,128)S(1)}, f32[128,2048]{0,1:T(8,128)}, u32[]{:S(2)}) copy-start(f32[128,2048]{0,1:T(8,128)} %copy-done.2) | copy-start | bytes 3145732
  1896.4 43.7 %copy-start.101 = (f32[127,2048]{0,1:T(8,128)S(1)}, f32[127,2048]{0,1:T(8,128)}, u32[]{:S(2)}) copy-start(f32[127,2048]{0,1:T(8,128)} %get-tuple-element.96) | copy-start | bytes 3121156
  2083.2 39.1 %copy-start.119 = (f32[128,2048]{0,1:T(8,128)S(1)}, f32[128,2048]{0,1:T(8,128)}, u32[]{:S(2)}) copy-start(f32[128,2048]{0,1:T(8,128)} %add.711) | copy-start | bytes 3145732
  2122.3 41.9 %copy-start.37 = (f32[256,2048]{0,1:T(8,128)}, f32[256,2048]{0,1:T(8,128)S(1)}, u32[]{:S(2)}) copy-start(f32[256,2048]{0,1:T(8,128)S(1)} %pad.256) | copy-start | bytes 6291460
  2167.1 39.2 %copy-start.113 = (f32[128,2048]{0,1:T(8,128)S(1)}, f32[128,2048]{0,1:T(8,128)}, u32[]{:S(2)}) copy-start(f32[128,2048]{0,1:T(8,128)} %add.709) | copy-start | bytes 3145732
  2206.4 41.7 %copy-start.38 = (f32[256,2048]{0,1:T(8,128)}, f32[256,2048]{0,1:T(8,128)S(1)}, u32[]{:S(2)}) copy-start(f32[256,2048]{0,1:T(8,128)S(1)} %pad.254) | copy-start | bytes 6291460
  2246.0 56.5 %copy-start.131 = (f32[2,1,32,64]{3,2,1,0:T(8,128)S(1)}, f32[2,1,32,64]{3,2,1,0:T(8,128)}, u32[]{:S(2)}) copy-start(f32[2,1,32,64]{3,2,1,0:T(8,128)} %param.33) | copy-start | bytes 49156
  2246.0 56.7 %copy-start.166 = (f32[256]{0:T(256)S(1)}, f32[256]{0:T(256)}, u32[]{:S(2)}) copy-start(f32[256]{0:T(256)} %copy-done.165) | copy-start | bytes 3076
  2246.0 56.7 %copy-start.168 = (f32[4096]{0:T(1024)S(1)}, f32[4096]{0:T(1024)}, u32[]{:S(2)}) copy-start(f32[4096]{0:T(1024)} %param.20) | copy-start | bytes 49156
  2311.2 11.2 collective-permute-start
  (144 other events, 507.0 us)
Sparse Core Ops, SparseCore 0:
  10.1 78.3 all-gather.11
  91.2 74.1 all-gather.7
  168.2 74.1 all-gather.5
  245.1 74.2 all-gather.9
  322.0 74.1 all-gather.13
  2338.8 9.8 reduce-scatter.1
where the time goes:
time: 2380 us; the launch traced here: 2360 us
  local copies, waits for them, and re-layouts  2050 us (86%)
  other arithmetic  173 us (7%)
  blocking collectives  54.2 us (2%)
  matrix products  41.3 us (2%)
    slice x85, local copies, waits for them, and re-layouts, body(): lax.associative_scan(link_states, (trans_re.reshape(row_count, flat_width...  1130 us
    pad x56, local copies, waits for them, and re-layouts, body(): lax.associative_scan(link_states, (trans_re.reshape(row_count, flat_width...  818 us
    all_gather x4, blocking collectives, carried_in(): gathered = jax.tree.map(lambda a: lax.all_gather(a, axis), part)  54.2 us
  transfers between devices with their start and end apart: 7, of which 1 were waited for; matrix products, arithmetic and copies ran while one was open for 95% of the time, Pallas kernels for 0%

commit v1 on v0

v1 whole, which is shorter than its diff:
```python
import functools

import jax
import jax.numpy as jnp
from jax import lax
from jax.experimental import pallas as pl
from jax.experimental.pallas import tpu as pltpu
from jax.sharding import PartitionSpec as P

HEAD_CH = 128
LANES = 128
CHUNKS = 8


def shifted(value, axis, steps):
    count = lax.axis_size(axis)
    initial, last = (max(0, -steps), min(count, count - steps))
    return lax.ppermute(value, axis, [(source, source + steps) for source in range(initial, last)])


def order_matrix(rows, transposed):
    length = rows // CHUNKS
    first = lax.broadcasted_iota(jnp.int32, (rows, rows), 0)
    second = lax.broadcasted_iota(jnp.int32, (rows, rows), 1)
    mixed, position = (second, first) if transposed else (first, second)
    hit = position == (mixed % CHUNKS) * length + mixed // CHUNKS
    return hit.astype(jnp.float32).astype(jnp.bfloat16)


def turn(angle):
    count = (angle * 0.6366197723675814 + 0.5).astype(jnp.int32)
    whole = count.astype(jnp.float32)
    rest = angle - whole * 1.5703125
    rest = rest - whole * 4.837512969970703125e-4
    rest = rest - whole * 7.54978995489188216e-8
    square = rest * rest
    sine = rest + rest * square * (
        -1.6666654611e-1 + square * (8.3321608736e-3 + square * -1.9515295891e-4)
    )
    less = square * (
        -0.5
        + square
        * (4.166664568298827e-2 + square * (-1.388731625493765e-3 + square * 2.443315711809948e-5))
    )
    cosine = 1.0 + less
    odd = (count & 1) == 1
    sin_out = jnp.where(odd, cosine, sine)
    cos_out = jnp.where(odd, sine, cosine)
    sin_out = jnp.where((count & 2) == 2, -sin_out, sin_out)
    cos_out = jnp.where(((count + 1) & 2) == 2, -cos_out, cos_out)
    less_out = jnp.where((count & 3) == 0, less, cos_out - 1.0)
    return less_out, cos_out, sin_out


def scan_kernel(
    x_ref, step_ref, spread_ref, lam_ref, high_ref, low_ref,
    are_ref, aim_ref, sre_ref, sim_ref, chunk_ref, total_ref,
    wide_ref, drive_ref,
):
    rows = x_ref.shape[0]
    width = lam_ref.shape[2]
    order = order_matrix(rows, False)
    x = jnp.dot(order, x_ref[...], preferred_element_type=jnp.float32).astype(jnp.bfloat16)
    drive_ref[...] = jnp.dot(x, high_ref[0], preferred_element_type=jnp.float32) + jnp.dot(
        x, low_ref[0], preferred_element_type=jnp.float32
    )
    wide_ref[...] = jnp.dot(
        step_ref[0], spread_ref[...], precision=lax.Precision.HIGHEST,
        preferred_element_type=jnp.float32,
    )

    def one(i, carry):
        here = pl.ds(pl.multiple_of(i * CHUNKS, CHUNKS), CHUNKS)
        results = []
        for j in range(width // LANES):
            a_re, a_im, s_re, s_im = carry[j]
            cols = slice(j * LANES, (j + 1) * LANES)
            step = wide_ref[here, cols]
            rate = lam_ref[0, 0:1, cols]
            freq = lam_ref[0, 1:2, cols]
            inv_re = lam_ref[0, 2:3, cols]
            inv_im = lam_ref[0, 3:4, cols]
            decay = -step * rate
            series = decay * (
                1.0 + decay * (0.5 + decay * (
                    1.0 / 6 + decay * (1.0 / 24 + decay * (1.0 / 120 + decay * (1.0 / 720)))
                ))
            )
            fall = jnp.where(decay > -0.25, series, jnp.exp(decay) - 1.0)
            modulus = 1.0 + fall
            modulus = jnp.where(decay > -0.25, modulus, jnp.exp(decay))
            cos_less, cosine, sine = turn(step * freq)
            t_re = modulus * cosine
            t_im = modulus * sine
            less = fall * cosine + cos_less
            f_re = less * inv_re - t_im * inv_im
            f_im = less * inv_im + t_im * inv_re
            d_re = drive_ref[here, cols]
            d_im = drive_ref[here, slice(width + j * LANES, width + (j + 1) * LANES)]
            p_re = f_re * d_re - f_im * d_im
            p_im = f_re * d_im + f_im * d_re
            s_re, s_im = t_re * s_re - t_im * s_im + p_re, t_re * s_im + t_im * s_re + p_im
            a_re, a_im = t_re * a_re - t_im * a_im, t_re * a_im + t_im * a_re
            are_ref[0, here, cols] = a_re
            aim_ref[0, here, cols] = a_im
            sre_ref[0, here, cols] = s_re
            sim_ref[0, here, cols] = s_im
            results.append((a_re, a_im, s_re, s_im))
        return tuple(results)

    ones = jnp.ones((CHUNKS, LANES), jnp.float32)
    zeros = jnp.zeros((CHUNKS, LANES), jnp.float32)
    start = tuple((ones, zeros, zeros, zeros) for _ in range(width // LANES))
    ends = lax.fori_loop(0, rows // CHUNKS, one, start)
    place = lax.broadcasted_iota(jnp.int32, (CHUNKS, LANES), 0)
    for j in range(width // LANES):
        cols = slice(j * LANES, (j + 1) * LANES)
        current = (ones[0:1], zeros[0:1], zeros[0:1], zeros[0:1])
        kept = [zeros] * 4
        for c in range(CHUNKS):
            kept = [jnp.where(place == c, v, k) for v, k in zip(current, kept)]
            t_re, t_im, p_re, p_im = (e[c : c + 1] for e in ends[j])
            a_re, a_im, s_re, s_im = current
            current = (
                t_re * a_re - t_im * a_im,
                t_re * a_im + t_im * a_re,
                t_re * s_re - t_im * s_im + p_re,
                t_re * s_im + t_im * s_re + p_im,
            )
        for q in range(4):
            chunk_ref[0, q, :, cols] = kept[q]
            total_ref[0, q : q + 1, cols] = current[q]


def read_kernel(
    are_ref, aim_ref, sre_ref, sim_ref, chunk_ref, enter_ref, x_ref, skip_ref, high_ref, low_ref,
    out_ref, state_ref,
):
    rows = x_ref.shape[0]
    width = are_ref.shape[2]
    e_re = enter_ref[0, 0:1, :]
    e_im = enter_ref[0, 1:2, :]
    a_re, a_im = chunk_ref[0, 0], chunk_ref[0, 1]
    c_re = a_re * e_re - a_im * e_im + chunk_ref[0, 2]
    c_im = a_re * e_im + a_im * e_re + chunk_ref[0, 3]

    def one(i, carry):
        here = pl.ds(pl.multiple_of(i * CHUNKS, CHUNKS), CHUNKS)
        a_re = are_ref[0, here, :]
        a_im = aim_ref[0, here, :]
        state_ref[here, 0:width] = sre_ref[0, here, :] + a_re * c_re - a_im * c_im
        state_ref[here, width : 2 * width] = sim_ref[0, here, :] + a_re * c_im + a_im * c_re
        return carry

    lax.fori_loop(0, rows // CHUNKS, one, 0)
    state = state_ref[...]
    high = state.astype(jnp.bfloat16)
    low = (state - high.astype(jnp.float32)).astype(jnp.bfloat16)
    read = (
        jnp.dot(high, high_ref[0], preferred_element_type=jnp.float32)
        + jnp.dot(low, high_ref[0], preferred_element_type=jnp.float32)
        + jnp.dot(high, low_ref[0], preferred_element_type=jnp.float32)
    )
    x = jnp.dot(order_matrix(rows, False), x_ref[...], preferred_element_type=jnp.float32)
    out = jax.nn.gelu(read + skip_ref[...] * x).astype(jnp.bfloat16)
    out_ref[...] = jnp.dot(
        order_matrix(rows, True), out, preferred_element_type=jnp.float32
    ).astype(jnp.bfloat16)


def conv_kernel_body(gated_ref, before_ref, taps_ref, gain_ref, out_ref, pad_ref):
    rows = gated_ref.shape[0]
    lead = before_ref.shape[0]
    count = taps_ref.shape[0]
    pad_ref[0:lead, :] = before_ref[...].astype(jnp.float32)
    pad_ref[lead:, :] = gated_ref[...].astype(jnp.float32)
    slab = 64
    for r in range(0, rows, slab):
        total = jnp.zeros((slab, LANES), jnp.float32)
        for k in range(count):
            begin = r + lead - (count - 1) + k
            total = total + taps_ref[k : k + 1, :] * pad_ref[begin : begin + slab, :]
        center = total - jnp.mean(total, axis=1, keepdims=True)
        spread = jnp.mean(center * center, axis=1, keepdims=True)
        value = center * lax.rsqrt(spread + 1e-05) * gain_ref[...]
        out_ref[r : r + slab, :] = (value * jax.nn.sigmoid(value)).astype(jnp.bfloat16)


def split(value):
    high = value.astype(jnp.bfloat16)
    low = (value - high.astype(jnp.float32)).astype(jnp.bfloat16)
    return high, low


def cost(flops, size):
    return pl.CostEstimate(flops=flops, bytes_accessed=size, transcendentals=0)


def body(
    stream, norm_gain, value_proj, gate_proj, state_proj, conv_kernel, conv_gain, decay_rate,
    frequency, log_step, step_gain, drive_matrix, read_matrix, skip_gain, start_state,
    merge_conv, merge_state,
):
    rows = stream.shape[1]
    groups, states = decay_rate.shape
    per = drive_matrix.shape[3]
    pack = min(groups, LANES // per)
    blocks = groups // pack
    width = pack * states
    chans = pack * per
    f32 = jnp.float32

    state_whole = lax.all_gather(state_proj, ("sp", "fs"), axis=0, tiled=True)
    value_whole = lax.all_gather(value_proj, ("sp", "fs"), axis=0, tiled=True)
    gate_whole = lax.all_gather(gate_proj, ("sp", "fs"), axis=0, tiled=True)
    conv_merge = lax.all_gather(merge_conv, ("sp", "fs"), axis=0, tiled=True)
    state_merge = lax.all_gather(merge_state, ("sp", "fs"), axis=0, tiled=True)

    widened = stream[0].astype(f32)
    inverse = lax.rsqrt(jnp.mean(widened * widened, axis=1, keepdims=True) + 1e-06)
    normed = (widened * inverse * norm_gain).astype(jnp.bfloat16)

    step = (jnp.exp(log_step)[:, None] * step_gain[0]).reshape(
        blocks, pack, CHUNKS, rows // CHUNKS
    )
    step = jnp.transpose(step, (0, 3, 2, 1)).reshape(blocks, rows, pack)
    spread = jnp.repeat(jnp.eye(pack, dtype=f32), states, axis=1)
    magnitude = decay_rate * decay_rate + frequency * frequency
    lam = jnp.stack(
        [decay_rate, frequency, -decay_rate / magnitude, -frequency / magnitude]
    ).reshape(4, blocks, width)
    lam = jnp.transpose(lam, (1, 0, 2))
    same = jnp.eye(pack, dtype=f32)
    drive = jnp.transpose(drive_matrix.reshape(2, blocks, pack, states, per), (1, 2, 4, 0, 3))
    drive = drive[:, :, :, :, None, :] * same[None, :, None, None, :, None]
    drive_high, drive_low = split(drive.reshape(blocks, chans, 2 * width))
    signed = jnp.stack([read_matrix[0], -read_matrix[1]])
    read = jnp.transpose(signed.reshape(2, blocks, pack, per, states), (1, 0, 2, 4, 3))
    read = read[:, :, :, :, None, :] * same[None, None, :, None, :, None]
    read_high, read_low = split(read.reshape(blocks, 2 * width, chans))

    scan_input = jnp.dot(normed, state_whole, preferred_element_type=f32).astype(jnp.bfloat16)

    def slab(*shape):
        return pl.BlockSpec((1,) + shape, lambda b: (b,) + (0,) * len(shape))

    chan_spec = pl.BlockSpec((rows, chans), lambda b: (0, b))
    row_spec = pl.BlockSpec((1, chans), lambda b: (0, b))
    wide = jax.ShapeDtypeStruct((blocks, rows, width), f32)
    *running, chunk, total = pl.pallas_call(
        scan_kernel,
        grid=(blocks,),
        in_specs=[
            chan_spec, slab(rows, pack), pl.BlockSpec((pack, width), lambda b: (0, 0)),
            slab(4, width), slab(chans, 2 * width), slab(chans, 2 * width),
        ],
        out_specs=[slab(rows, width)] * 4 + [slab(4, CHUNKS, width), slab(4, width)],
        out_shape=[wide] * 4 + [
            jax.ShapeDtypeStruct((blocks, 4, CHUNKS, width), f32),
            jax.ShapeDtypeStruct((blocks, 4, width), f32),
        ],
        scratch_shapes=[pltpu.VMEM((rows, width), f32), pltpu.VMEM((rows, 2 * width), f32)],
        cost_estimate=cost(60 * rows * blocks * width * 30, 16 * rows * blocks * width),
        name="scan",
    )(scan_input, step, spread, lam, drive_high, drive_low)

    place = lax.axis_index("sp")
    arrived = [
        (hop, shifted(total, "sp", hop)) for hop in range(lax.axis_size("sp") - 1, 0, -1)
    ]
    begin = start_state[:, 0].reshape(2, blocks, width)
    enter_re, enter_im = begin[0], begin[1]
    for hop, part in arrived:
        t_re, t_im, p_re, p_im = (part[:, q] for q in range(4))
        known = place >= hop
        next_re = t_re * enter_re - t_im * enter_im + p_re
        next_im = t_re * enter_im + t_im * enter_re + p_im
        enter_re = jnp.where(known, next_re, enter_re)
        enter_im = jnp.where(known, next_im, enter_im)
    enter = jnp.stack([enter_re, enter_im], axis=1)

    state_out = pl.pallas_call(
        read_kernel,
        grid=(blocks,),
        in_specs=[slab(rows, width)] * 4 + [
            slab(4, CHUNKS, width), slab(2, width), chan_spec, row_spec,
            slab(2 * width, chans), slab(2 * width, chans),
        ],
        out_specs=chan_spec,
        out_shape=jax.ShapeDtypeStruct((rows, groups * per), jnp.bfloat16),
        scratch_shapes=[pltpu.VMEM((rows, 2 * width), f32)],
        cost_estimate=cost(60 * rows * blocks * width * 10, 16 * rows * blocks * width),
        name="read",
    )(*running, chunk, enter, scan_input, skip_gain[None], read_high, read_low)

    value_pre = jnp.dot(normed, value_whole, preferred_element_type=f32)
    gate_pre = jnp.dot(normed, gate_whole, preferred_element_type=f32)
    gated = (value_pre * jax.nn.sigmoid(gate_pre)).astype(jnp.bfloat16)
    lead = -(-(conv_kernel.shape[0] - 1) // 16) * 16
    before = shifted(gated[rows - lead :], "sp", 1)
    conv_width = gated.shape[1]
    head_spec = lambda n: pl.BlockSpec((n, HEAD_CH), lambda h: (0, h))
    conv_out = pl.pallas_call(
        conv_kernel_body,
        grid=(conv_width // HEAD_CH,),
        in_specs=[
            head_spec(rows), head_spec(lead), head_spec(conv_kernel.shape[0]), head_spec(1),
        ],
        out_specs=head_spec(rows),
        out_shape=jax.ShapeDtypeStruct((rows, conv_width), jnp.bfloat16),
        scratch_shapes=[pltpu.VMEM((rows + lead, HEAD_CH), f32)],
        cost_estimate=cost(rows * conv_width * 2000, 4 * rows * conv_width),
        name="conv",
    )(gated, before, conv_kernel.astype(f32), conv_gain[None])

    contract = (((1,), (1,)), ((), ()))
    conv_term = lax.dot_general(conv_out, conv_merge, contract, preferred_element_type=f32)
    state_term = lax.dot_general(state_out, state_merge, contract, preferred_element_type=f32)
    mixed = lax.psum_scatter(
        (conv_term + state_term).astype(jnp.bfloat16), "tp", scatter_dimension=0, tiled=True
    )
    return mixed[None]


def solution(mesh):
    return jax.shard_map(
        body,
        mesh=mesh,
        in_specs=(
            P("fs", "sp", None),
            P(),
            P(("sp", "fs"), "tp"),
            P(("sp", "fs"), "tp"),
            P(("sp", "fs"), "tp"),
            P(None, "tp"),
            P("tp"),
            P("tp", None),
            P("tp", None),
            P("tp"),
            P("fs", "tp", "sp"),
            P(None, "tp", None, None),
            P(None, "tp", None, None),
            P("tp"),
            P(None, "fs", "tp", None),
            P(("sp", "fs"), "tp"),
            P(("sp", "fs"), "tp"),
        ),
        out_specs=P("fs", ("sp", "tp"), None),
        check_vma=False,
    )
```

time: 2380 us -> 418 us (0.18)
  local copies, waits for them, and re-layouts: 2050 us -> 23.8 us
  waiting for transfers between devices: 13.3 us -> 310 us
  other arithmetic: 173 us -> 9.6 us
  blocking collectives: 54.2 us -> 0 us
  Pallas kernels: 0 us -> 26.7 us
    slice x88 -> x2, local copies, waits for them, and re-layouts: 1130 us -> 0.01 us  [the longest x1 0.01 us: body(): before = shifted(gated[rows - lead:], 'sp', 1)]
    pad x56 -> x0, local copies, waits for them, and re-layouts: 818 us -> none  [body(): lax.associative_scan(link_states, (trans_re.reshape(row_count, flat_width...]
    all_gather x5, waiting for transfers between devices: 0.07 us -> 297 us  [the longest x1 73.4 us: body(): value_whole = lax.all_gather(value_proj, ('sp', 'fs'), axis=0, tiled=True)]
    add x51 -> x0, other arithmetic: 87.8 us -> none  [the longest x26 46.7 us: body(): lax.associative_scan(link_states, (trans_re.reshape(row_count, flat_width...]
    all_gather x4 -> x0, blocking collectives: 54.2 us -> none  [carried_in(): gathered = jax.tree.map(lambda a: lax.all_gather(a, axis), part)]
    unnamed x356 -> x30, local copies, waits for them, and re-layouts: 46.9 us -> 0.66 us
    concatenate x28 -> x0, other arithmetic: 30.5 us -> none  [body(): lax.associative_scan(link_states, (trans_re.reshape(row_count, flat_width...]
    pallas_call x0 -> x3, Pallas kernels: none -> 26.7 us  [the longest x1 15 us: body(): pl.pallas_call(scan_kernel, grid=(blocks,), in_specs=[chan_spec, slab(row...]
  transfers between devices with their start and end apart: 7 -> 10, of which waited for: 1 -> 7; matrix products, arithmetic and copies ran while one was open for 95% -> 12% of each run, Pallas kernels for 0% -> 6%
where the time goes in v1:
time: 418 us
  waiting for transfers between devices  310 us (74%)
  Pallas kernels  26.7 us (6%)
  local copies, waits for them, and re-layouts  23.8 us (6%)
  matrix products  22.9 us (5%)
  between operations  13.7 us (3%)
  starting transfers between devices  11.4 us (3%)
  other arithmetic  9.6 us (2%)
    all_gather x1, waiting for transfers between devices, body(): value_whole = lax.all_gather(value_proj, ('sp', 'fs'), axis=0, tiled=True)  73.4 us
    all_gather x1, waiting for transfers between devices, body(): conv_merge = lax.all_gather(merge_conv, ('sp', 'fs'), axis=0, tiled=True)  71.3 us
    all_gather x1, waiting for transfers between devices, body(): state_merge = lax.all_gather(merge_state, ('sp', 'fs'), axis=0, tiled=True)  55.3 us
    all_gather x1, waiting for transfers between devices, body(): gate_whole = lax.all_gather(gate_proj, ('sp', 'fs'), axis=0, tiled=True)  50.2 us
    all_gather x1, waiting for transfers between devices, body(): state_whole = lax.all_gather(state_proj, ('sp', 'fs'), axis=0, tiled=True)  46.4 us
    pallas_call x1, Pallas kernels, body(): pl.pallas_call(scan_kernel, grid=(blocks,), in_specs=[chan_spec, slab(row...  15 us
    mul x6, local copies, waits for them, and re-layouts, body(): read = read[:, :, :, :, None, :] * same[None, None, :, None, :, None]  12.9 us
    ppermute x4, starting transfers between devices, shifted(): lax.ppermute(value, axis, [(source, source + steps) for source in range(i...  11.2 us
  transfers between devices with their start and end apart: 10, of which 7 were waited for; matrix products, arithmetic and copies ran while one was open for 12% of the time, Pallas kernels for 6%

profile of v1, /device:TPU:0, one launch (start us, length us, event | category | flops | bytes accessed | tf_op | source)
XLA Modules:
  0.0 417.7 jit_solution(12097990945348739648)
XLA Ops:
  10.2 1.1 mul.149
  11.7 2.3 mul.146
  14.1 3.6 mul.147
  18.8 1.0 copy.21
  20.4 2.5 mul.164
  22.9 4.9 %mul.165 = f32[4,1024,128]{1,2,0:T(8,128)} reshape(f32[4,2,8,64,8,16]{3,2,1,5,4,0:T(8,128)} %mul.164) | data formatting | bytes 4194304 | tf_op jit(solution)/shard_map/mul | solution.py:239
  27.8 3.0 copy.27
  30.9 1.1 mul.167
  32.0 1.3 copy.26
  34.6 2.1 fusion.1
  36.7 1.9 multiply_bitcast_fusion.step_ref
  38.6 1.8 subtract_convert_fusion.1
  40.4 1.7 subtract_convert_fusion
  42.1 46.4 %all-gather.12.cloned.1.call-done = bf16[4096,512]{1,0:T(8,128)(2,1)} async-done(((bf16[256,512]{1,0:T(8,128)(2,1)}), bf16[4096,512]{1,0:T(8,128)(2,1)}) %all-gather.12.cloned.1.call-update) | async-done | bytes 4194320 | tf_op jit(solution)/shard_map/all_gather | solution.py:213
  88.5 4.2 %convolution_convert_fusion.x_ref = bf16[256,512]{1,0:T(8,128)(2,1)} fusion(bf16[4096,512]{1,0:T(8,128)(2,1)} %all-gather.12.cloned.1.call-done, bf16[1,256,4096]{2,1,0:T(8,128)(2,1)S(1)} %copy-done.2, f32[4096]{0:T(1024)S(1)} %copy-done.13, f32[256]{0:T(256)S(1)} %add_rsqrt_fusion), kind=kOutput, calls=%fused_computation.17 | convolution fusion | flops 1078067200 | bytes 6571008 | tf_op jit(solution)/shard_map/dot_general | solution.py:242
  92.6 15.0 %scan.1 = (f32[4,256,512]{2,1,0:T(8,128)}, f32[4,256,512]{2,1,0:T(8,128)}, f32[4,256,512]{2,1,0:T(8,128)}, f32[4,256,512]{2,1,0:T(8,128)}, f32[4,4,8,512]{3,2,1,0:T(8,128)}, /*index=5*/f32[4,4,512]{2,1,0:T(4,128)}) custom-call(bf16[256,512]{1,0:T(8,128)(2,1)} %convolution_convert_fusion.x_ref, f32[4,256,8]{2,1,0:T(8,128)} %multiply_bitcast_fusion.step_ref, ...), custom_call_target="tpu_custom_call" | custom-call | flops 943718400 | bytes 8388608 | tf_op jit(solution)/shard_map/scan/pallas_call | solution.py:250
  107.6 3.8 collective-permute-start.3
  111.5 1.3 collective-permute-start.1
  112.8 2.5 collective-permute-start.2
  115.2 50.2 %all-gather.8.cloned.1.call-done = bf16[4096,512]{1,0:T(8,128)(2,1)} async-done(((bf16[256,512]{1,0:T(8,128)(2,1)}), bf16[4096,512]{1,0:T(8,128)(2,1)}) %all-gather.8.cloned.1.call-update) | async-done | bytes 4194320 | tf_op jit(solution)/shard_map/all_gather | solution.py:215
  165.5 3.5 fusion.6
  169.0 73.4 %all-gather.6.cloned.1.call-done = bf16[4096,512]{1,0:T(8,128)(2,1)} async-done(((bf16[256,512]{1,0:T(8,128)(2,1)}), bf16[4096,512]{1,0:T(8,128)(2,1)}) %all-gather.6.cloned.1.call-update) | async-done | bytes 4194320 | tf_op jit(solution)/shard_map/all_gather | solution.py:214
  242.5 3.5 fusion.7.gated_ref
  246.0 3.6 collective-permute-start
  249.6 1.3 collective-permute-done.before_ref
  251.6 4.0 conv.1
  256.3 7.7 %read.1 = bf16[256,512]{1,0:T(8,128)(2,1)} custom-call(f32[4,256,512]{2,1,0:T(8,128)} %get-tuple-element.11.are_ref, f32[4,256,512]{2,1,0:T(8,128)} %get-tuple-element.12.aim_ref, f32[4,256,512]{2,1,0:T(8,128)} %get-tuple-element.13.sre_ref, f32[4,256,512]{2,1,0:T(8,128)} %get-tuple-element.14.sim_ref, f32[4,4,8,512]{3,2,1,0:T(8,128)} %get-tuple-element.15.chunk_ref, ...), custom_call_target="tpu_custom_call" | custom-call | flops 314572800 | bytes 8388608 | tf_op jit(solution)/shard_map/read/pallas_call | solution.py:282
  264.0 55.3 %all-gather.14.cloned.1.call-done = bf16[4096,512]{1,0:T(8,128)(2,1)} async-done(((bf16[256,512]{1,0:T(8,128)(2,1)}), bf16[4096,512]{1,0:T(8,128)(2,1)}) %all-gather.14.cloned.1.call-update) | async-done | bytes 4194320 | tf_op jit(solution)/shard_map/all_gather | solution.py:217
  319.3 5.6 %fusion.14 = f32[256,4096]{1,0:T(8,128)} fusion(bf16[256,512]{1,0:T(8,128)(2,1)} %read.1, bf16[4096,512]{1,0:T(8,128)(2,1)} %all-gather.14.cloned.1.call-done), kind=kOutput, calls=%fused_computation.43 | convolution fusion | flops 1073741824 | bytes 8650752 | tf_op jit(solution)/shard_map/dot_general | solution.py:318
  324.9 71.3 %all-gather.10.cloned.1.call-done = bf16[4096,512]{1,0:T(8,128)(2,1)} async-done(((bf16[256,512]{1,0:T(8,128)(2,1)}), bf16[4096,512]{1,0:T(8,128)(2,1)}) %all-gather.10.cloned.1.call-update) | async-done | bytes 4194320 | tf_op jit(solution)/shard_map/all_gather | solution.py:216
  396.2 6.1 %fusion = bf16[256,4096]{1,0:T(8,128)(2,1)} fusion(f32[256,4096]{1,0:T(8,128)} %fusion.14, bf16[256,512]{1,0:T(8,128)(2,1)S(1)} %copy-done.5, bf16[4096,512]{1,0:T(8,128)(2,1)} %all-gather.10.cloned.1.call-done), kind=kOutput, calls=%fused_computation.3 | convolution fusion | flops 1075838976 | bytes 10747904 | tf_op jit(solution)/shard_map/dot_general | solution.py:317
  402.3 8.5 %reduce-scatter.2.cloned.1.call-done = bf16[128,4096]{1,0:T(8,128)(2,1)} async-done(((bf16[256,4096]{1,0:T(8,128)(2,1)}), bf16[128,4096]{1,0:T(8,128)(2,1)}) %reduce-scatter.2.cloned.1.call-update) | async-done | bytes 1048592 | tf_op jit(solution)/shard_map/reduce_scatter | solution.py:319
  (74 shorter events, 8.4 us)
Async XLA Ops:
  6.5 4.8 %copy-start.3 = (f32[2,32,64,16]{2,3,1,0:T(8,128)S(1)}, f32[2,32,64,16]{2,3,1,0:T(8,128)}, u32[]{:S(2)}) copy-start(f32[2,32,64,16]{2,3,1,0:T(8,128)} %param.28) | copy-start | bytes 786436
  6.5 81.9 %all-gather.12.cloned.1.call-start = ((), (), s32[]{:S(2)}) async-start(), calls=%async_computation.4 | async-start | bytes 4456448 | tf_op jit(solution)/shard_map/all_gather | solution.py:213
  7.3 158.2 %all-gather.8.cloned.1.call-start = ((), (), s32[]{:S(2)}) async-start(), calls=%async_computation.2 | async-start | bytes 4456448 | tf_op jit(solution)/shard_map/all_gather | solution.py:215
  8.0 234.5 %all-gather.6.cloned.1.call-start = ((), (), s32[]{:S(2)}) async-start(), calls=%async_computation.1 | async-start | bytes 4456448 | tf_op jit(solution)/shard_map/all_gather | solution.py:214
  8.7 310.6 %all-gather.14.cloned.1.call-start = ((), (), s32[]{:S(2)}) async-start(), calls=%async_computation.5 | async-start | bytes 4456448 | tf_op jit(solution)/shard_map/all_gather | solution.py:217
  9.3 386.9 %all-gather.10.cloned.1.call-start = ((), (), s32[]{:S(2)}) async-start(), calls=%async_computation.3 | async-start | bytes 4456448 | tf_op jit(solution)/shard_map/all_gather | solution.py:216
  9.9 401.0 %reduce-scatter.2.cloned.1.call-start = ((), (), s32[]{:S(2)}) async-start(), calls=%async_computation.6 | async-start | bytes 3145728 | tf_op jit(solution)/shard_map/reduce_scatter | solution.py:319
  14.1 3.6 copy-start.6
  14.1 3.7 copy-start.7
  14.1 4.7 %copy-start.8 = (f32[1,32,256]{2,1,0:T(8,128)S(1)}, f32[1,32,256]{2,1,0:T(8,128)}, u32[]{:S(2)}) copy-start(f32[1,32,256]{2,1,0:T(8,128)} %param.27) | copy-start | bytes 98308
  14.1 5.8 %copy-start.14 = (f32[32]{0:T(128)S(1)}, f32[32]{0:T(128)}, u32[]{:S(2)}) copy-start(f32[32]{0:T(128)} %param.26) | copy-start | bytes 388
  14.1 5.9 %copy-start.10 = (f32[2,1,32,64]{3,2,1,0:T(8,128)S(1)}, f32[2,1,32,64]{3,2,1,0:T(8,128)}, u32[]{:S(2)}) copy-start(f32[2,1,32,64]{3,2,1,0:T(8,128)} %param.31) | copy-start | bytes 49156
  14.1 6.1 %copy-start.4 = (f32[2,32,16,64]{3,2,1,0:T(8,128)S(1)}, f32[2,32,16,64]{3,2,1,0:T(8,128)}, u32[]{:S(2)}) copy-start(f32[2,32,16,64]{3,2,1,0:T(8,128)} %param.29) | copy-start | bytes 786436
  27.8 5.5 %copy-start.9 = (bf16[31,512]{1,0:T(8,128)(2,1)S(1)}, bf16[31,512]{1,0:T(8,128)(2,1)}, u32[]{:S(2)}) copy-start(bf16[31,512]{1,0:T(8,128)(2,1)} %param.22) | copy-start | bytes 95236
  32.0 6.6 %copy-start.1 = (f32[128,1024]{1,0:T(8,128)S(1)}, f32[128,1024]{1,0:T(8,128)}, u32[]{:S(2)}) copy-start(f32[128,1024]{1,0:T(8,128)} %mul.149) | copy-start | bytes 1572868
  33.3 7.0 %copy-start = (f32[4,1024,128]{2,1,0:T(8,128)S(1)}, f32[4,1024,128]{2,1,0:T(8,128)}, u32[]{:S(2)}) copy-start(f32[4,1024,128]{2,1,0:T(8,128)} %copy.27) | copy-start | bytes 6291460
  38.6 49.9 %copy-start.13 = (f32[4096]{0:T(1024)S(1)}, f32[4096]{0:T(1024)}, u32[]{:S(2)}) copy-start(f32[4096]{0:T(1024)} %param.18) | copy-start | bytes 49156
  40.3 48.1 %copy-start.2 = (bf16[1,256,4096]{2,1,0:T(8,128)(2,1)S(1)}, bf16[1,256,4096]{2,1,0:T(8,128)(2,1)}, u32[]{:S(2)}) copy-start(bf16[1,256,4096]{2,1,0:T(8,128)(2,1)} %param.17) | copy-start | bytes 6291460
  107.6 141.9 %collective-permute-start.3 = (f32[4,4,512]{2,1,0:T(4,128)}, f32[4,4,512]{2,1,0:T(4,128)S(1)}, u32[]{:S(2)}, u32[]{:S(2)}) collective-permute-start(f32[4,4,512]{2,1,0:T(4,128)} %get-tuple-element.16), channel_id=1, source_target_pairs={{0,24},{1,25},{2,26},{3,27},{4,28},{5,29},{6,30},{7,31}} | collective-permute-start | bytes 98312 | tf_op jit(solution)/shard_map/ppermute | solution.py:18
  111.5 144.1 %collective-permute-start.1 = (f32[4,4,512]{2,1,0:T(4,128)}, f32[4,4,512]{2,1,0:T(4,128)S(1)}, u32[]{:S(2)}, u32[]{:S(2)}) collective-permute-start(f32[4,4,512]{2,1,0:T(4,128)} %get-tuple-element.16), channel_id=1, source_target_pairs={{0,8},{8,16},{16,24},{1,9},{9,17},{17,25},{2,10},{10,18},{18,26},{... | collective-permute-start | bytes 98312 | tf_op jit(solution)/shard_map/ppermute | solution.py:18
  112.8 142.8 %collective-permute-start.2 = (f32[4,4,512]{2,1,0:T(4,128)}, f32[4,4,512]{2,1,0:T(4,128)S(1)}, u32[]{:S(2)}, u32[]{:S(2)}) collective-permute-start(f32[4,4,512]{2,1,0:T(4,128)} %get-tuple-element.16), channel_id=1, source_target_pairs={{0,16},{8,24},{1,17},{9,25},{2,18},{10,26},{3,19},{11,27},{4,20},{... | collective-permute-start | bytes 98312 | tf_op jit(solution)/shard_map/ppermute | solution.py:18
  246.0 5.0 %copy-start.11 = (bf16[256,512]{1,0:T(8,128)(2,1)}, bf16[256,512]{1,0:T(8,128)(2,1)S(1)}, u32[]{:S(2)}) copy-start(bf16[256,512]{1,0:T(8,128)(2,1)S(1)} %fusion.7.gated_ref) | copy-start | bytes 786436
  246.0 5.0 %collective-permute-start = (bf16[32,512]{1,0:T(8,128)(2,1)S(1)}, bf16[32,512]{1,0:T(8,128)(2,1)S(1)}, u32[]{:S(2)}, u32[]{:S(2)}) collective-permute-start(bf16[32,512]{1,0:T(8,128)(2,1)S(1)} %slice.70), channel_id=1, source_target_pairs={{0,8},{8,16},{16,24},{1,9},{9,17},{17,25},{2,10},{10,18},{18,26},{... | collective-permute-start | bytes 98312 | tf_op jit(solution)/shard_map/ppermute | solution.py:18
  251.0 0.6 copy-start.12
  264.0 132.2 %copy-start.5 = (bf16[256,512]{1,0:T(8,128)(2,1)S(1)}, bf16[256,512]{1,0:T(8,128)(2,1)}, u32[]{:S(2)}) copy-start(bf16[256,512]{1,0:T(8,128)(2,1)} %conv.1) | copy-start | bytes 786436
Sparse Core Ops, SparseCore 0:
  10.1 78.3 all-gather.11
  91.2 74.2 all-gather.7
  168.3 74.1 all-gather.5
  245.1 74.1 all-gather.13
  321.9 74.1 all-gather.9
  402.5 8.3 reduce-scatter.1

commit v2 on v1

--- a/solution.py
+++ b/solution.py
@@ -196,6 +196,103 @@
     return pl.CostEstimate(flops=flops, bytes_accessed=size, transcendentals=0)
 
 
+def ring_order(p, n):
+    if n != 4:
+        return p
+    return p + lax.div(p, 2) * (1 - 2 * lax.rem(p, 2))
+
+
+def gather_kernel(sizes, own_ref, out_ref, send_sem, recv_sem, local_sem):
+    rows = own_ref.shape[0]
+    s = lax.axis_index("sp")
+    f = lax.axis_index("fs")
+    spots = {"sp": s, "fs": ring_order(f, sizes["fs"])}
+
+    def index(axis, position):
+        return position if axis == "sp" else ring_order(position, sizes["fs"])
+
+    def neighbours(axis):
+        n, me = sizes[axis], spots[axis]
+        return lax.rem(me + 1, n), lax.rem(me + n - 1, n)
+
+    barrier = pltpu.get_barrier_semaphore()
+    for axis in ("sp", "fs"):
+        for position in neighbours(axis):
+            pl.semaphore_signal(
+                barrier, inc=1, device_id={axis: index(axis, position)},
+                device_id_type=pl.DeviceIdType.MESH,
+            )
+    pl.semaphore_wait(barrier, 4)
+
+    local = pltpu.make_async_copy(own_ref, out_ref.at[s, f], local_sem)
+    local.start()
+    started = []
+
+    def hop(axis, phase, half, h):
+        n, me = sizes[axis], spots[axis]
+        base, size = half * (rows // 2), rows // 2
+        if 2 * h == n:
+            spans = ((base, size // 2), (base + size // 2, size // 2))
+        else:
+            spans = ((base, size), (base, size))
+        blocks = (lax.rem(me + n - (h - 1), n), lax.rem(me + h - 1, n))
+        copies = []
+        for position, block, span in zip(neighbours(axis), blocks, spans):
+            where = pl.ds(*span)
+            at = index(axis, block)
+            if phase == 0:
+                view = out_ref.at[at, f, where] if axis == "sp" else out_ref.at[s, at, where]
+            else:
+                view = out_ref.at[at, :, where] if axis == "sp" else out_ref.at[:, at, where]
+            slot = len(started)
+            copy = pltpu.make_async_remote_copy(
+                src_ref=own_ref.at[where] if phase == 0 and h == 1 else view,
+                dst_ref=view,
+                send_sem=send_sem.at[slot],
+                recv_sem=recv_sem.at[slot],
+                device_id={axis: index(axis, position)},
+                device_id_type=pl.DeviceIdType.MESH,
+            )
+            copy.start()
+            started.append(copy)
+            copies.append(copy)
+        return copies
+
+    for phase in range(2):
+        routes = (("sp", "fs")[phase], 0), (("fs", "sp")[phase], 1)
+        if phase == 1:
+            local.wait()
+        for h in range(1, max(sizes.values()) // 2 + 1):
+            flying = []
+            for axis, half in routes:
+                if h <= sizes[axis] // 2:
+                    flying += hop(axis, phase, half, h)
+            for copy in flying:
+                copy.wait_recv()
+    for copy in started:
+        copy.wait_send()
+
+
+def gathered_rows(own):
+    sizes = {axis: lax.axis_size(axis) for axis in ("sp", "fs")}
+    copies = 4 * sum(n // 2 for n in sizes.values())
+    out = pl.pallas_call(
+        functools.partial(gather_kernel, sizes),
+        in_specs=[pl.BlockSpec(memory_space=pl.ANY)],
+        out_specs=pl.BlockSpec(memory_space=pl.ANY),
+        out_shape=jax.ShapeDtypeStruct((sizes["sp"], sizes["fs"]) + own.shape, own.dtype),
+        scratch_shapes=[
+            pltpu.SemaphoreType.DMA((copies,)),
+            pltpu.SemaphoreType.DMA((copies,)),
+            pltpu.SemaphoreType.DMA,
+        ],
+        compiler_params=pltpu.CompilerParams(collective_id=0, has_side_effects=True),
+        cost_estimate=cost(10**6, 100 * own.size),
+        name="gather",
+    )(own)
+    return out.reshape(-1, own.shape[1])
+
+
 def body(
     stream, norm_gain, value_proj, gate_proj, state_proj, conv_kernel, conv_gain, decay_rate,
     frequency, log_step, step_gain, drive_matrix, read_matrix, skip_gain, start_state,
@@ -210,9 +307,7 @@
     chans = pack * per
     f32 = jnp.float32
 
-    state_whole = lax.all_gather(state_proj, ("sp", "fs"), axis=0, tiled=True)
-    value_whole = lax.all_gather(value_proj, ("sp", "fs"), axis=0, tiled=True)
-    gate_whole = lax.all_gather(gate_proj, ("sp", "fs"), axis=0, tiled=True)
+    proj_whole = gathered_rows(jnp.concatenate([state_proj, value_proj, gate_proj], axis=1))
     conv_merge = lax.all_gather(merge_conv, ("sp", "fs"), axis=0, tiled=True)
     state_merge = lax.all_gather(merge_state, ("sp", "fs"), axis=0, tiled=True)
 
@@ -239,7 +334,9 @@
     read = read[:, :, :, :, None, :] * same[None, None, :, None, :, None]
     read_high, read_low = split(read.reshape(blocks, 2 * width, chans))
 
-    scan_input = jnp.dot(normed, state_whole, preferred_element_type=f32).astype(jnp.bfloat16)
+    pre = jnp.dot(normed, proj_whole, preferred_element_type=f32)
+    scan_width, conv_width = state_proj.shape[1], value_proj.shape[1]
+    scan_input = pre[:, :scan_width].astype(jnp.bfloat16)
 
     def slab(*shape):
         return pl.BlockSpec((1,) + shape, lambda b: (b,) + (0,) * len(shape))
@@ -293,12 +390,11 @@
         name="read",
     )(*running, chunk, enter, scan_input, skip_gain[None], read_high, read_low)
 
-    value_pre = jnp.dot(normed, value_whole, preferred_element_type=f32)
-    gate_pre = jnp.dot(normed, gate_whole, preferred_element_type=f32)
+    value_pre = pre[:, scan_width : scan_width + conv_width]
+    gate_pre = pre[:, scan_width + conv_width :]
     gated = (value_pre * jax.nn.sigmoid(gate_pre)).astype(jnp.bfloat16)
     lead = -(-(conv_kernel.shape[0] - 1) // 16) * 16
     before = shifted(gated[rows - lead :], "sp", 1)
-    conv_width = gated.shape[1]
     head_spec = lambda n: pl.BlockSpec((n, HEAD_CH), lambda h: (0, h))
     conv_out = pl.pallas_call(
         conv_kernel_body,

time: 418 us -> 291 us (0.70)
  waiting for transfers between devices: 310 us -> 10.6 us
  Pallas kernels: 26.7 us -> 207 us
  matrix products: 22.9 us -> 18.4 us
    pallas_call x0 -> x1, Pallas kernels: none -> 180 us  [gathered_rows(): pl.pallas_call(functools.partial(gather_kernel, sizes), in_specs=[pl.Bloc...]
    all_gather x3 -> x0, waiting for transfers between devices: 170 us -> none  [the longest x1 73.4 us: body(): value_whole = lax.all_gather(value_proj, ('sp', 'fs'), axis=0, tiled=True)]
    all_gather x1, waiting for transfers between devices: 71.3 us -> 0.01 us  [body(): conv_merge = lax.all_gather(merge_conv, ('sp', 'fs'), axis=0, tiled=True)]
    all_gather x1, waiting for transfers between devices: 55.3 us -> 0.02 us  [body(): state_merge = lax.all_gather(merge_state, ('sp', 'fs'), axis=0, tiled=True)]
    dot_general x3 -> x1, matrix products: 11.2 us -> 6.74 us  [body(): pre = jnp.dot(normed, proj_whole, preferred_element_type=f32)]
  transfers between devices with their start and end apart: 10 -> 7, of which waited for: 7 -> 1; matrix products, arithmetic and copies ran while one was open for 12% -> 14% of each run, Pallas kernels for 6% -> 71%
where the time goes in v2:
time: 291 us
  Pallas kernels  207 us (71%)
  local copies, waits for them, and re-layouts  20.8 us (7%)
  matrix products  18.4 us (6%)
  between operations  13.5 us (5%)
  waiting for transfers between devices  10.6 us (4%)
  starting transfers between devices  10.5 us (4%)
  other arithmetic  9.68 us (3%)
    pallas_call x1, Pallas kernels, gathered_rows(): pl.pallas_call(functools.partial(gather_kernel, sizes), in_specs=[pl.Bloc...  180 us
    pallas_call x1, Pallas kernels, body(): pl.pallas_call(scan_kernel, grid=(blocks,), in_specs=[chan_spec, slab(row...  15.2 us
    ppermute x4, starting transfers between devices, shifted(): lax.ppermute(value, axis, [(source, source + steps) for source in range(i...  10.5 us
    mul x6, local copies, waits for them, and re-layouts, body(): read = read[:, :, :, :, None, :] * same[None, None, :, None, :, None]  10.3 us
    reduce_scatter x1, waiting for transfers between devices, body(): lax.psum_scatter((conv_term + state_term).astype(jnp.bfloat16), 'tp', sca...  9.13 us
    pallas_call x1, Pallas kernels, body(): pl.pallas_call(read_kernel, grid=(blocks,), in_specs=[slab(rows, width)]...  7.7 us
    dot_general x1, matrix products, body(): pre = jnp.dot(normed, proj_whole, preferred_element_type=f32)  6.74 us
    mul x4, local copies, waits for them, and re-layouts, body(): drive = drive[:, :, :, :, None, :] * same[None, :, None, None, :, None]  6.28 us
  transfers between devices with their start and end apart: 7, of which 1 were waited for; matrix products, arithmetic and copies ran while one was open for 14% of the time, Pallas kernels for 71%

profile of v2, /device:TPU:0, one launch (start us, length us, event | category | flops | bytes accessed | tf_op | source)
XLA Modules:
  0.0 290.8 jit_solution(5956845050117795932)
XLA Ops:
  6.5 0.7 all-gather.5.cloned.1.call-update
  7.3 0.7 all-gather.3.cloned.1.call-update
  9.0 2.3 mul.149
  11.3 3.6 %mul.150 = f32[4,128,1024]{2,1,0:T(8,128)S(1)} reshape(f32[4,8,16,2,8,64]{5,4,3,2,1,0:T(8,128)} %mul.149) | data formatting | bytes 4194304 | tf_op jit(solution)/shard_map/mul | solution.py:330
  14.9 0.9 pad_maximum_fusion.own_ref
  15.8 180.4 %gather.1 = bf16[4,4,256,1536]{3,2,1,0:T(8,128)(2,1)} custom-call(bf16[256,1536]{1,0:T(8,128)(2,1)} %pad_maximum_fusion.own_ref), custom_call_target="tpu_custom_call" | custom-call | flops 1000000 | bytes 39321600 | tf_op jit(solution)/shard_map/gather/pallas_call | solution.py:279
  196.2 2.2 fusion.1
  198.5 6.7 %fusion.5 = f32[256,1536]{1,0:T(8,128)S(1)} fusion(bf16[4096,1536]{1,0:T(8,128)(2,1)} %bitcast.41, bf16[1,256,4096]{2,1,0:T(8,128)(2,1)S(1)} %copy-done.1, f32[4096]{0:T(1024)S(1)} %copy-done.16, f32[256]{0:T(256)S(1)} %add_rsqrt_fusion), kind=kOutput, calls=%fused_computation.8 | convolution fusion | flops 3225419776 | bytes 16270336 | tf_op jit(solution)/shard_map/dot_general | solution.py:337
  205.3 1.2 copy-done.2
  206.5 0.7 slice.145.x_ref
  207.6 0.7 reshape.91.spread_ref
  208.7 0.6 maximum_bitcast_fusion.1.lam_ref
  209.4 0.8 multiply_bitcast_fusion.step_ref
  210.2 1.8 subtract_convert_fusion.1
  212.0 15.2 %scan.1 = (f32[4,256,512]{2,1,0:T(8,128)}, f32[4,256,512]{2,1,0:T(8,128)}, f32[4,256,512]{2,1,0:T(8,128)}, f32[4,256,512]{2,1,0:T(8,128)}, f32[4,4,8,512]{3,2,1,0:T(8,128)}, /*index=5*/f32[4,4,512]{2,1,0:T(4,128)}) custom-call(bf16[256,512]{1,0:T(8,128)(2,1)} %slice.145.x_ref, f32[4,256,8]{2,1,0:T(8,128)} %multiply_bitcast_fusion.step_ref, ...), custom_call_target="tpu_custom_call" | custom-call | flops 943718400 | bytes 8388608 | tf_op jit(solution)/shard_map/scan/pallas_call | solution.py:347
  227.1 4.8 %collective-permute-start.3 = (f32[4,4,512]{2,1,0:T(4,128)}, f32[4,4,512]{2,1,0:T(4,128)S(1)}, u32[]{:S(2)}, u32[]{:S(2)}) collective-permute-start(f32[4,4,512]{2,1,0:T(4,128)} %get-tuple-element.16), channel_id=1, source_target_pairs={{0,24},{1,25},{2,26},{3,27},{4,28},{5,29},{6,30},{7,31}} | collective-permute-start | bytes 98312 | tf_op jit(solution)/shard_map/ppermute | solution.py:18
  232.0 1.3 collective-permute-start.1
  233.3 2.5 collective-permute-start.2
  235.9 1.9 collective-permute-start
  238.1 2.4 mul.167
  240.5 3.5 %mul.168 = f32[4,1024,128]{1,2,0:T(8,128)S(1)} reshape(f32[4,2,8,64,8,16]{3,2,1,5,4,0:T(8,128)} %mul.167) | data formatting | bytes 4194304 | tf_op jit(solution)/shard_map/mul | solution.py:334
  244.0 1.9 copy.27
  246.0 1.1 mul.170
  247.1 1.2 copy.26
  248.4 1.7 subtract_convert_fusion
  250.2 0.6 convert_element_type.59.taps_ref
  250.9 4.0 %conv.1 = bf16[256,512]{1,0:T(8,128)(2,1)} custom-call(bf16[256,512]{1,0:T(8,128)(2,1)} %copy-done.6, bf16[32,512]{1,0:T(8,128)(2,1)} %collective-permute-done.before_ref, f32[31,512]{1,0:T(8,128)} %convert_element_type.59.taps_ref, f32[1,512]{1,0:T(1,128)} %bitcast.46), custom_call_target="tpu_custom_call" | custom-call | flops 262144000 | bytes 524288 | tf_op jit(solution)/shard_map/conv/pallas_call | solution.py:399
  255.0 0.6 pad_maximum_fusion.1.enter_ref
  255.7 7.7 %read.1 = bf16[256,512]{1,0:T(8,128)(2,1)} custom-call(f32[4,256,512]{2,1,0:T(8,128)} %get-tuple-element.11.are_ref, f32[4,256,512]{2,1,0:T(8,128)} %get-tuple-element.12.aim_ref, f32[4,256,512]{2,1,0:T(8,128)} %get-tuple-element.13.sre_ref, f32[4,256,512]{2,1,0:T(8,128)} %get-tuple-element.14.sim_ref, f32[4,4,8,512]{3,2,1,0:T(8,128)} %get-tuple-element.15.chunk_ref, ...), custom_call_target="tpu_custom_call" | custom-call | flops 314572800 | bytes 8388608 | tf_op jit(solution)/shard_map/read/pallas_call | solution.py:379
  263.4 5.6 %fusion.17 = f32[256,4096]{1,0:T(8,128)} fusion(bf16[256,512]{1,0:T(8,128)(2,1)} %read.1, bf16[4096,512]{1,0:T(8,128)(2,1)} %all-gather.5.cloned.1.call-done), kind=kOutput, calls=%fused_computation.48 | convolution fusion | flops 1073741824 | bytes 8650752 | tf_op jit(solution)/shard_map/dot_general | solution.py:414
  268.9 6.1 %fusion = bf16[256,4096]{1,0:T(8,128)(2,1)} fusion(f32[256,4096]{1,0:T(8,128)} %fusion.17, bf16[256,512]{1,0:T(8,128)(2,1)S(1)} %copy-done.10, bf16[4096,512]{1,0:T(8,128)(2,1)} %all-gather.3.cloned.1.call-done), kind=kOutput, calls=%fused_computation.3 | convolution fusion | flops 1075838976 | bytes 10747904 | tf_op jit(solution)/shard_map/dot_general | solution.py:413
  275.1 9.1 %reduce-scatter.2.cloned.1.call-done = bf16[128,4096]{1,0:T(8,128)(2,1)} async-done(((bf16[256,4096]{1,0:T(8,128)(2,1)}), bf16[128,4096]{1,0:T(8,128)(2,1)}) %reduce-scatter.2.cloned.1.call-update) | async-done | bytes 1048592 | tf_op jit(solution)/shard_map/reduce_scatter | solution.py:415
  (73 shorter events, 2.8 us)
Async XLA Ops:
  6.5 2.1 copy-start.4
  6.5 256.8 %all-gather.5.cloned.1.call-start = ((), (), s32[]{:S(2)}) async-start(), calls=%async_computation.2 | async-start | bytes 4456448 | tf_op jit(solution)/shard_map/all_gather | solution.py:312
  7.3 261.7 %all-gather.3.cloned.1.call-start = ((), (), s32[]{:S(2)}) async-start(), calls=%async_computation.1 | async-start | bytes 4456448 | tf_op jit(solution)/shard_map/all_gather | solution.py:311
  8.0 276.2 %reduce-scatter.2.cloned.1.call-start = ((), (), s32[]{:S(2)}) async-start(), calls=%async_computation.3 | async-start | bytes 3145728 | tf_op jit(solution)/shard_map/reduce_scatter | solution.py:415
  11.3 3.6 %copy-start.7 = (bf16[256,512]{1,0:T(8,128)(2,1)S(1)}, bf16[256,512]{1,0:T(8,128)(2,1)}, u32[]{:S(2)}) copy-start(bf16[256,512]{1,0:T(8,128)(2,1)} %param.20) | copy-start | bytes 786436
  11.3 3.6 %copy-start.8 = (bf16[256,512]{1,0:T(8,128)(2,1)S(1)}, bf16[256,512]{1,0:T(8,128)(2,1)}, u32[]{:S(2)}) copy-start(bf16[256,512]{1,0:T(8,128)(2,1)} %param.19) | copy-start | bytes 786436
  11.3 3.6 %copy-start.9 = (bf16[256,512]{1,0:T(8,128)(2,1)S(1)}, bf16[256,512]{1,0:T(8,128)(2,1)}, u32[]{:S(2)}) copy-start(bf16[256,512]{1,0:T(8,128)(2,1)} %param.21) | copy-start | bytes 786436
  15.8 182.6 %copy-start.16 = (f32[4096]{0:T(1024)S(1)}, f32[4096]{0:T(1024)}, u32[]{:S(2)}) copy-start(f32[4096]{0:T(1024)} %param.18) | copy-start | bytes 49156
  196.2 2.3 copy-start.1
  198.5 8.7 %copy-start.11 = (f32[32,64]{1,0:T(8,128)S(1)}, f32[32,64]{1,0:T(8,128)}, u32[]{:S(2)}) copy-start(f32[32,64]{1,0:T(8,128)} %param.24) | copy-start | bytes 24580
  198.5 8.8 %copy-start.12 = (f32[32,64]{1,0:T(8,128)S(1)}, f32[32,64]{1,0:T(8,128)}, u32[]{:S(2)}) copy-start(f32[32,64]{1,0:T(8,128)} %param.25) | copy-start | bytes 24580
  198.5 9.8 %copy-start.13 = (f32[1,32,256]{2,1,0:T(8,128)S(1)}, f32[1,32,256]{2,1,0:T(8,128)}, u32[]{:S(2)}) copy-start(f32[1,32,256]{2,1,0:T(8,128)} %param.27) | copy-start | bytes 98308
  198.5 10.1 %copy-start.17 = (f32[32]{0:T(128)S(1)}, f32[32]{0:T(128)}, u32[]{:S(2)}) copy-start(f32[32]{0:T(128)} %param.26) | copy-start | bytes 388
  205.3 1.2 copy-start.2
  212.0 23.8 %copy-start.3 = (f32[256,1536]{1,0:T(8,128)S(1)}, f32[256,1536]{1,0:T(8,128)}, u32[]{:S(2)}) copy-start(f32[256,1536]{1,0:T(8,128)} %copy-done.2) | copy-start | bytes 4718596
  212.0 25.8 %copy-start.5 = (f32[2,32,16,64]{3,2,1,0:T(8,128)S(1)}, f32[2,32,16,64]{3,2,1,0:T(8,128)}, u32[]{:S(2)}) copy-start(f32[2,32,16,64]{3,2,1,0:T(8,128)} %param.29) | copy-start | bytes 786436
  227.1 23.7 %collective-permute-start.3 = (f32[4,4,512]{2,1,0:T(4,128)}, f32[4,4,512]{2,1,0:T(4,128)S(1)}, u32[]{:S(2)}, u32[]{:S(2)}) collective-permute-start(f32[4,4,512]{2,1,0:T(4,128)} %get-tuple-element.16), channel_id=1, source_target_pairs={{0,24},{1,25},{2,26},{3,27},{4,28},{5,29},{6,30},{7,31}} | collective-permute-start | bytes 98312 | tf_op jit(solution)/shard_map/ppermute | solution.py:18
  232.0 23.0 %collective-permute-start.1 = (f32[4,4,512]{2,1,0:T(4,128)}, f32[4,4,512]{2,1,0:T(4,128)S(1)}, u32[]{:S(2)}, u32[]{:S(2)}) collective-permute-start(f32[4,4,512]{2,1,0:T(4,128)} %get-tuple-element.16), channel_id=1, source_target_pairs={{0,8},{8,16},{16,24},{1,9},{9,17},{17,25},{2,10},{10,18},{18,26},{... | collective-permute-start | bytes 98312 | tf_op jit(solution)/shard_map/ppermute | solution.py:18
  233.3 21.7 %collective-permute-start.2 = (f32[4,4,512]{2,1,0:T(4,128)}, f32[4,4,512]{2,1,0:T(4,128)S(1)}, u32[]{:S(2)}, u32[]{:S(2)}) collective-permute-start(f32[4,4,512]{2,1,0:T(4,128)} %get-tuple-element.16), channel_id=1, source_target_pairs={{0,16},{8,24},{1,17},{9,25},{2,18},{10,26},{3,19},{11,27},{4,20},{... | collective-permute-start | bytes 98312 | tf_op jit(solution)/shard_map/ppermute | solution.py:18
  235.9 4.6 %copy-start.6 = (bf16[256,512]{1,0:T(8,128)(2,1)}, bf16[256,512]{1,0:T(8,128)(2,1)S(1)}, u32[]{:S(2)}) copy-start(bf16[256,512]{1,0:T(8,128)(2,1)S(1)} %fusion.13.gated_ref) | copy-start | bytes 786436
  235.9 15.0 %collective-permute-start = (bf16[32,512]{1,0:T(8,128)(2,1)S(1)}, bf16[32,512]{1,0:T(8,128)(2,1)}, u32[]{:S(2)}, u32[]{:S(2)}) collective-permute-start(bf16[32,512]{1,0:T(8,128)(2,1)S(1)} %slice.85), channel_id=1, source_target_pairs={{0,8},{8,16},{16,24},{1,9},{9,17},{17,25},{2,10},{10,18},{18,26},{... | collective-permute-start | bytes 98312 | tf_op jit(solution)/shard_map/ppermute | solution.py:18
  245.9 2.5 copy-start
  248.4 1.7 copy-start.15
  248.4 1.9 copy-start.14
  263.4 5.6 %copy-start.10 = (bf16[256,512]{1,0:T(8,128)(2,1)S(1)}, bf16[256,512]{1,0:T(8,128)(2,1)}, u32[]{:S(2)}) copy-start(bf16[256,512]{1,0:T(8,128)(2,1)} %conv.1) | copy-start | bytes 786436
Sparse Core Ops, SparseCore 0:
  10.1 141.2 all-gather.4
  154.1 96.2 all-gather.2
  275.2 8.9 reduce-scatter.1

commit v3 on v2

--- a/solution.py
+++ b/solution.py
@@ -52,8 +52,16 @@
     return less_out, cos_out, sin_out
 
 
+def spread_groups(compact, pack, per):
+    chans, states = compact.shape
+    wide = jnp.concatenate([compact] * pack, axis=1)
+    row = lax.broadcasted_iota(jnp.int32, wide.shape, 0) // per
+    column = lax.broadcasted_iota(jnp.int32, wide.shape, 1) // states
+    return jnp.where(row == column, wide, 0.0)
+
+
 def scan_kernel(
-    x_ref, step_ref, spread_ref, lam_ref, high_ref, low_ref,
+    x_ref, step_ref, spread_ref, lam_ref, matrix_ref,
     are_ref, aim_ref, sre_ref, sim_ref, chunk_ref, total_ref,
     wide_ref, drive_ref,
 ):
@@ -61,9 +69,12 @@
     width = lam_ref.shape[2]
     order = order_matrix(rows, False)
     x = jnp.dot(order, x_ref[...], preferred_element_type=jnp.float32).astype(jnp.bfloat16)
-    drive_ref[...] = jnp.dot(x, high_ref[0], preferred_element_type=jnp.float32) + jnp.dot(
-        x, low_ref[0], preferred_element_type=jnp.float32
-    )
+    pack = step_ref.shape[2]
+    for q in range(2):
+        high, low = split(spread_groups(matrix_ref[q, 0], pack, x_ref.shape[1] // pack))
+        drive_ref[:, q * width : (q + 1) * width] = jnp.dot(
+            x, high, preferred_element_type=jnp.float32
+        ) + jnp.dot(x, low, preferred_element_type=jnp.float32)
     wide_ref[...] = jnp.dot(
         step_ref[0], spread_ref[...], precision=lax.Precision.HIGHEST,
         preferred_element_type=jnp.float32,
@@ -133,7 +144,7 @@
 
 
 def read_kernel(
-    are_ref, aim_ref, sre_ref, sim_ref, chunk_ref, enter_ref, x_ref, skip_ref, high_ref, low_ref,
+    are_ref, aim_ref, sre_ref, sim_ref, chunk_ref, enter_ref, x_ref, skip_ref, matrix_ref,
     out_ref, state_ref,
 ):
     rows = x_ref.shape[0]
@@ -153,14 +164,15 @@
         return carry
 
     lax.fori_loop(0, rows // CHUNKS, one, 0)
-    state = state_ref[...]
-    high = state.astype(jnp.bfloat16)
-    low = (state - high.astype(jnp.float32)).astype(jnp.bfloat16)
-    read = (
-        jnp.dot(high, high_ref[0], preferred_element_type=jnp.float32)
-        + jnp.dot(low, high_ref[0], preferred_element_type=jnp.float32)
-        + jnp.dot(high, low_ref[0], preferred_element_type=jnp.float32)
-    )
+    pack = width // matrix_ref.shape[3]
+    reads = []
+    for q in range(2):
+        high, low = split(state_ref[:, q * width : (q + 1) * width])
+        major, minor = split(spread_groups(matrix_ref[q, 0], pack, x_ref.shape[1] // pack))
+        reads.append(
+            across(high, major) + across(low, major) + across(high, minor)
+        )
+    read = reads[0] - reads[1]
     x = jnp.dot(order_matrix(rows, False), x_ref[...], preferred_element_type=jnp.float32)
     out = jax.nn.gelu(read + skip_ref[...] * x).astype(jnp.bfloat16)
     out_ref[...] = jnp.dot(
@@ -186,6 +198,12 @@
         out_ref[r : r + slab, :] = (value * jax.nn.sigmoid(value)).astype(jnp.bfloat16)
 
 
+def across(left, right):
+    return lax.dot_general(
+        left, right, (((1,), (1,)), ((), ())), preferred_element_type=jnp.float32
+    )
+
+
 def split(value):
     high = value.astype(jnp.bfloat16)
     low = (value - high.astype(jnp.float32)).astype(jnp.bfloat16)
@@ -230,7 +248,8 @@
 
     def hop(axis, phase, half, h):
         n, me = sizes[axis], spots[axis]
-        base, size = half * (rows // 2), rows // 2
+        cut = rows * 5 // 8 // 32 * 32
+        base, size = ((0, cut), (cut, rows - cut))[half]
         if 2 * h == n:
             spans = ((base, size // 2), (base + size // 2, size // 2))
         else:
@@ -325,14 +344,8 @@
         [decay_rate, frequency, -decay_rate / magnitude, -frequency / magnitude]
     ).reshape(4, blocks, width)
     lam = jnp.transpose(lam, (1, 0, 2))
-    same = jnp.eye(pack, dtype=f32)
-    drive = jnp.transpose(drive_matrix.reshape(2, blocks, pack, states, per), (1, 2, 4, 0, 3))
-    drive = drive[:, :, :, :, None, :] * same[None, :, None, None, :, None]
-    drive_high, drive_low = split(drive.reshape(blocks, chans, 2 * width))
-    signed = jnp.stack([read_matrix[0], -read_matrix[1]])
-    read = jnp.transpose(signed.reshape(2, blocks, pack, per, states), (1, 0, 2, 4, 3))
-    read = read[:, :, :, :, None, :] * same[None, None, :, None, :, None]
-    read_high, read_low = split(read.reshape(blocks, 2 * width, chans))
+    drive = jnp.swapaxes(drive_matrix, 2, 3).reshape(2, blocks, chans, states)
+    read = read_matrix.reshape(2, blocks, chans, states)
 
     pre = jnp.dot(normed, proj_whole, preferred_element_type=f32)
     scan_width, conv_width = state_proj.shape[1], value_proj.shape[1]
@@ -341,6 +354,7 @@
     def slab(*shape):
         return pl.BlockSpec((1,) + shape, lambda b: (b,) + (0,) * len(shape))
 
+    pair_spec = pl.BlockSpec((2, 1, chans, states), lambda b: (0, b, 0, 0))
     chan_spec = pl.BlockSpec((rows, chans), lambda b: (0, b))
     row_spec = pl.BlockSpec((1, chans), lambda b: (0, b))
     wide = jax.ShapeDtypeStruct((blocks, rows, width), f32)
@@ -349,7 +363,7 @@
         grid=(blocks,),
         in_specs=[
             chan_spec, slab(rows, pack), pl.BlockSpec((pack, width), lambda b: (0, 0)),
-            slab(4, width), slab(chans, 2 * width), slab(chans, 2 * width),
+            slab(4, width), pair_spec,
         ],
         out_specs=[slab(rows, width)] * 4 + [slab(4, CHUNKS, width), slab(4, width)],
         out_shape=[wide] * 4 + [
@@ -359,7 +373,7 @@
         scratch_shapes=[pltpu.VMEM((rows, width), f32), pltpu.VMEM((rows, 2 * width), f32)],
         cost_estimate=cost(60 * rows * blocks * width * 30, 16 * rows * blocks * width),
         name="scan",
-    )(scan_input, step, spread, lam, drive_high, drive_low)
+    )(scan_input, step, spread, lam, drive)
 
     place = lax.axis_index("sp")
     arrived = [
@@ -381,14 +395,14 @@
         grid=(blocks,),
         in_specs=[slab(rows, width)] * 4 + [
             slab(4, CHUNKS, width), slab(2, width), chan_spec, row_spec,
-            slab(2 * width, chans), slab(2 * width, chans),
+            pair_spec,
         ],
         out_specs=chan_spec,
         out_shape=jax.ShapeDtypeStruct((rows, groups * per), jnp.bfloat16),
         scratch_shapes=[pltpu.VMEM((rows, 2 * width), f32)],
         cost_estimate=cost(60 * rows * blocks * width * 10, 16 * rows * blocks * width),
         name="read",
-    )(*running, chunk, enter, scan_input, skip_gain[None], read_high, read_low)
+    )(*running, chunk, enter, scan_input, skip_gain[None], read)
 
     value_pre = pre[:, scan_width : scan_width + conv_width]
     gate_pre = pre[:, scan_width + conv_width :]

time: 291 us -> 256 us (0.88)
  Pallas kernels: 207 us -> 189 us
  local copies, waits for them, and re-layouts: 20.8 us -> 4.24 us
  waiting for transfers between devices: 10.6 us -> 15.2 us
  other arithmetic: 9.68 us -> 5.53 us
    pallas_call x1, Pallas kernels: 180 us -> 162 us  [gathered_rows(): pl.pallas_call(functools.partial(gather_kernel, sizes), in_specs=[pl.Bloc...]
    mul x10 -> x0, local copies, waits for them, and re-layouts: 16.5 us -> none  [the longest x6 10.3 us: body(): read = read[:, :, :, :, None, :] * same[None, None, :, None, :, None]]
    convert_element_type x2 -> x0, other arithmetic: 3.44 us -> none  [split(): low = (value - high.astype(jnp.float32)).astype(jnp.bfloat16)]
    reduce_scatter x1, waiting for transfers between devices: 9.13 us -> 12.4 us  [body(): lax.psum_scatter((conv_term + state_term).astype(jnp.bfloat16), 'tp', sca...]
  transfers between devices with their start and end apart: 7 -> 7, of which waited for: 1 -> 2; matrix products, arithmetic and copies ran while one was open for 14% -> 8% of each run, Pallas kernels for 71% -> 74%
where the time goes in v3:
time: 256 us
  Pallas kernels  189 us (74%)
  matrix products  18.2 us (7%)
  waiting for transfers between devices  15.2 us (6%)
  between operations  13.3 us (5%)
  starting transfers between devices  10.5 us (4%)
  other arithmetic  5.53 us (2%)
  local copies, waits for them, and re-layouts  4.24 us (2%)
    pallas_call x1, Pallas kernels, gathered_rows(): pl.pallas_call(functools.partial(gather_kernel, sizes), in_specs=[pl.Bloc...  162 us
    pallas_call x1, Pallas kernels, body(): pl.pallas_call(scan_kernel, grid=(blocks,), in_specs=[chan_spec, slab(row...  14.9 us
    reduce_scatter x1, waiting for transfers between devices, body(): lax.psum_scatter((conv_term + state_term).astype(jnp.bfloat16), 'tp', sca...  12.4 us
    ppermute x4, starting transfers between devices, shifted(): lax.ppermute(value, axis, [(source, source + steps) for source in range(i...  10.4 us
    pallas_call x1, Pallas kernels, body(): pl.pallas_call(read_kernel, grid=(blocks,), in_specs=[slab(rows, width)]...  7.59 us
    dot_general x1, matrix products, body(): pre = jnp.dot(normed, proj_whole, preferred_element_type=f32)  6.54 us
    dot_general x1, matrix products, body(): lax.dot_general(conv_out, conv_merge, contract, preferred_element_type=f32)  6.11 us
    dot_general x1, matrix products, body(): lax.dot_general(state_out, state_merge, contract, preferred_element_type=...  5.54 us
  transfers between devices with their start and end apart: 7, of which 2 were waited for; matrix products, arithmetic and copies ran while one was open for 8% of the time, Pallas kernels for 74%

profile of v3, /device:TPU:0, one launch (start us, length us, event | category | flops | bytes accessed | tf_op | source)
XLA Modules:
  0.0 255.8 jit_solution(6097853849942929877)
XLA Ops:
  6.5 0.7 all-gather.5.cloned.1.call-update
  7.3 0.7 all-gather.3.cloned.1.call-update
  8.1 2.0 pad_maximum_fusion.own_ref
  10.1 162.3 %gather.1 = bf16[4,4,256,1536]{3,2,1,0:T(8,128)(2,1)} custom-call(bf16[256,1536]{1,0:T(8,128)(2,1)} %pad_maximum_fusion.own_ref), custom_call_target="tpu_custom_call" | custom-call | flops 1000000 | bytes 39321600 | tf_op jit(solution)/shard_map/gather/pallas_call | solution.py:298
  172.4 0.5 fusion.1
  173.0 6.5 %fusion.5 = f32[256,1536]{1,0:T(8,128)S(1)} fusion(bf16[4096,1536]{1,0:T(8,128)(2,1)} %bitcast.26, bf16[1,256,4096]{2,1,0:T(8,128)(2,1)S(1)} %copy-done, f32[4096]{0:T(1024)S(1)} %copy-done.11, f32[256]{0:T(256)S(1)} %add_rsqrt_fusion), kind=kOutput, calls=%fused_computation.8 | convolution fusion | flops 3225419776 | bytes 16270336 | tf_op jit(solution)/shard_map/dot_general | solution.py:350
  179.6 1.2 copy-done.1
  180.7 0.7 slice.136.x_ref
  181.6 0.1 stack.21
  181.7 0.1 stack.22
  181.8 0.1 squeeze.6
  181.9 0.3 copy.18
  182.2 0.1 mul.104
  182.4 0.7 reshape.67.spread_ref
  183.0 0.6 maximum_bitcast_fusion.lam_ref
  183.7 0.8 multiply_bitcast_fusion.step_ref
  184.5 14.9 %scan.1 = (f32[4,256,512]{2,1,0:T(8,128)}, f32[4,256,512]{2,1,0:T(8,128)}, f32[4,256,512]{2,1,0:T(8,128)}, f32[4,256,512]{2,1,0:T(8,128)}, f32[4,4,8,512]{3,2,1,0:T(8,128)}, /*index=5*/f32[4,4,512]{2,1,0:T(4,128)}) custom-call(bf16[256,512]{1,0:T(8,128)(2,1)} %slice.136.x_ref, f32[4,256,8]{2,1,0:T(8,128)} %multiply_bitcast_fusion.step_ref, ...), custom_call_target="tpu_custom_call" | custom-call | flops 943718400 | bytes 8388608 | tf_op jit(solution)/shard_map/scan/pallas_call | solution.py:361
  199.4 3.1 %collective-permute-start.3 = (f32[4,4,512]{2,1,0:T(4,128)}, f32[4,4,512]{2,1,0:T(4,128)S(1)}, u32[]{:S(2)}, u32[]{:S(2)}) collective-permute-start(f32[4,4,512]{2,1,0:T(4,128)} %get-tuple-element.16), channel_id=1, source_target_pairs={{0,24},{1,25},{2,26},{3,27},{4,28},{5,29},{6,30},{7,31}} | collective-permute-start | bytes 98312 | tf_op jit(solution)/shard_map/ppermute | solution.py:18
  202.6 1.6 collective-permute-start.1
  204.2 3.8 %collective-permute-start.2 = (f32[4,4,512]{2,1,0:T(4,128)}, f32[4,4,512]{2,1,0:T(4,128)S(1)}, u32[]{:S(2)}, u32[]{:S(2)}) collective-permute-start(f32[4,4,512]{2,1,0:T(4,128)} %get-tuple-element.16), channel_id=1, source_target_pairs={{0,16},{8,24},{1,17},{9,25},{2,18},{10,26},{3,19},{11,27},{4,20},{... | collective-permute-start | bytes 98312 | tf_op jit(solution)/shard_map/ppermute | solution.py:18
  208.1 0.1 fusion.13.gated_ref
  208.2 1.8 collective-permute-start
  210.1 0.1 squeeze.7
  210.3 0.6 convert_element_type.28.taps_ref
  211.0 1.4 collective-permute-done.before_ref
  212.3 0.6 copy-done.10
  212.9 4.0 %conv.1 = bf16[256,512]{1,0:T(8,128)(2,1)} custom-call(bf16[256,512]{1,0:T(8,128)(2,1)} %copy-done.3, bf16[32,512]{1,0:T(8,128)(2,1)} %copy-done.10, f32[31,512]{1,0:T(8,128)} %convert_element_type.28.taps_ref, f32[1,512]{1,0:T(1,128)} %bitcast.30), custom_call_target="tpu_custom_call" | custom-call | flops 262144000 | bytes 524288 | tf_op jit(solution)/shard_map/conv/pallas_call | solution.py:413
  217.0 0.6 pad_maximum_fusion.1.enter_ref
  217.6 7.6 %read.1 = bf16[256,512]{1,0:T(8,128)(2,1)} custom-call(f32[4,256,512]{2,1,0:T(8,128)} %get-tuple-element.11.are_ref, f32[4,256,512]{2,1,0:T(8,128)} %get-tuple-element.12.aim_ref, f32[4,256,512]{2,1,0:T(8,128)} %get-tuple-element.13.sre_ref, f32[4,256,512]{2,1,0:T(8,128)} %get-tuple-element.14.sim_ref, f32[4,4,8,512]{3,2,1,0:T(8,128)} %get-tuple-element.15.chunk_ref, ...), custom_call_target="tpu_custom_call" | custom-call | flops 314572800 | bytes 8388608 | tf_op jit(solution)/shard_map/read/pallas_call | solution.py:393
  225.2 5.5 %fusion.16 = f32[256,4096]{1,0:T(8,128)} fusion(bf16[256,512]{1,0:T(8,128)(2,1)} %read.1, bf16[4096,512]{1,0:T(8,128)(2,1)} %all-gather.5.cloned.1.call-done), kind=kOutput, calls=%fused_computation.41 | convolution fusion | flops 1073741824 | bytes 8650752 | tf_op jit(solution)/shard_map/dot_general | solution.py:428
  230.8 6.1 %fusion = bf16[256,4096]{1,0:T(8,128)(2,1)} fusion(f32[256,4096]{1,0:T(8,128)} %fusion.16, bf16[256,512]{1,0:T(8,128)(2,1)S(1)} %copy-done.4, bf16[4096,512]{1,0:T(8,128)(2,1)} %all-gather.3.cloned.1.call-done), kind=kOutput, calls=%fused_computation.3 | convolution fusion | flops 1075838976 | bytes 10747904 | tf_op jit(solution)/shard_map/dot_general | solution.py:427
  236.9 12.4 %reduce-scatter.2.cloned.1.call-done = bf16[128,4096]{1,0:T(8,128)(2,1)} async-done(((bf16[256,4096]{1,0:T(8,128)(2,1)}), bf16[128,4096]{1,0:T(8,128)(2,1)}) %reduce-scatter.2.cloned.1.call-update) | async-done | bytes 1048592 | tf_op jit(solution)/shard_map/reduce_scatter | solution.py:429
  (46 shorter events, 0.7 us)
Async XLA Ops:
  6.5 218.7 %all-gather.5.cloned.1.call-start = ((), (), s32[]{:S(2)}) async-start(), calls=%async_computation.2 | async-start | bytes 4456448 | tf_op jit(solution)/shard_map/all_gather | solution.py:331
  7.3 223.5 %all-gather.3.cloned.1.call-start = ((), (), s32[]{:S(2)}) async-start(), calls=%async_computation.1 | async-start | bytes 4456448 | tf_op jit(solution)/shard_map/all_gather | solution.py:330
  8.0 241.3 %reduce-scatter.2.cloned.1.call-start = ((), (), s32[]{:S(2)}) async-start(), calls=%async_computation.3 | async-start | bytes 3145728 | tf_op jit(solution)/shard_map/reduce_scatter | solution.py:429
  10.1 162.3 %copy-start = (bf16[1,256,4096]{2,1,0:T(8,128)(2,1)S(1)}, bf16[1,256,4096]{2,1,0:T(8,128)(2,1)}, u32[]{:S(2)}) copy-start(bf16[1,256,4096]{2,1,0:T(8,128)(2,1)} %param.17) | copy-start | bytes 6291460
  10.1 162.9 %copy-start.11 = (f32[4096]{0:T(1024)S(1)}, f32[4096]{0:T(1024)}, u32[]{:S(2)}) copy-start(f32[4096]{0:T(1024)} %param.18) | copy-start | bytes 49156
  173.0 8.5 %copy-start.5 = (f32[32,64]{1,0:T(8,128)S(1)}, f32[32,64]{1,0:T(8,128)}, u32[]{:S(2)}) copy-start(f32[32,64]{1,0:T(8,128)} %param.24) | copy-start | bytes 24580
  173.0 8.6 %copy-start.6 = (f32[32,64]{1,0:T(8,128)S(1)}, f32[32,64]{1,0:T(8,128)}, u32[]{:S(2)}) copy-start(f32[32,64]{1,0:T(8,128)} %param.25) | copy-start | bytes 24580
  173.0 8.8 %copy-start.7 = (f32[1,32,256]{2,1,0:T(8,128)S(1)}, f32[1,32,256]{2,1,0:T(8,128)}, u32[]{:S(2)}) copy-start(f32[1,32,256]{2,1,0:T(8,128)} %param.27) | copy-start | bytes 98308
  173.0 9.2 %copy-start.12 = (f32[32]{0:T(128)S(1)}, f32[32]{0:T(128)}, u32[]{:S(2)}) copy-start(f32[32]{0:T(128)} %param.26) | copy-start | bytes 388
  179.5 1.2 copy-start.1
  180.7 29.4 %copy-start.9 = (f32[2,1,32,64]{3,2,1,0:T(8,128)S(1)}, f32[2,1,32,64]{3,2,1,0:T(8,128)}, u32[]{:S(2)}) copy-start(f32[2,1,32,64]{3,2,1,0:T(8,128)} %param.31) | copy-start | bytes 49156
  180.7 29.5 %copy-start.8 = (bf16[31,512]{1,0:T(8,128)(2,1)S(1)}, bf16[31,512]{1,0:T(8,128)(2,1)}, u32[]{:S(2)}) copy-start(bf16[31,512]{1,0:T(8,128)(2,1)} %param.22) | copy-start | bytes 95236
  181.5 26.6 %copy-start.2 = (f32[256,1536]{1,0:T(8,128)S(1)}, f32[256,1536]{1,0:T(8,128)}, u32[]{:S(2)}) copy-start(f32[256,1536]{1,0:T(8,128)} %copy-done.1) | copy-start | bytes 4718596
  199.4 11.5 %collective-permute-start.3 = (f32[4,4,512]{2,1,0:T(4,128)}, f32[4,4,512]{2,1,0:T(4,128)S(1)}, u32[]{:S(2)}, u32[]{:S(2)}) collective-permute-start(f32[4,4,512]{2,1,0:T(4,128)} %get-tuple-element.16), channel_id=1, source_target_pairs={{0,24},{1,25},{2,26},{3,27},{4,28},{5,29},{6,30},{7,31}} | collective-permute-start | bytes 98312 | tf_op jit(solution)/shard_map/ppermute | solution.py:18
  202.6 14.3 %collective-permute-start.1 = (f32[4,4,512]{2,1,0:T(4,128)}, f32[4,4,512]{2,1,0:T(4,128)S(1)}, u32[]{:S(2)}, u32[]{:S(2)}) collective-permute-start(f32[4,4,512]{2,1,0:T(4,128)} %get-tuple-element.16), channel_id=1, source_target_pairs={{0,8},{8,16},{16,24},{1,9},{9,17},{17,25},{2,10},{10,18},{18,26},{... | collective-permute-start | bytes 98312 | tf_op jit(solution)/shard_map/ppermute | solution.py:18
  204.2 12.7 %collective-permute-start.2 = (f32[4,4,512]{2,1,0:T(4,128)}, f32[4,4,512]{2,1,0:T(4,128)S(1)}, u32[]{:S(2)}, u32[]{:S(2)}) collective-permute-start(f32[4,4,512]{2,1,0:T(4,128)} %get-tuple-element.16), channel_id=1, source_target_pairs={{0,16},{8,24},{1,17},{9,25},{2,18},{10,26},{3,19},{11,27},{4,20},{... | collective-permute-start | bytes 98312 | tf_op jit(solution)/shard_map/ppermute | solution.py:18
  208.2 4.1 %copy-start.3 = (bf16[256,512]{1,0:T(8,128)(2,1)}, bf16[256,512]{1,0:T(8,128)(2,1)S(1)}, u32[]{:S(2)}) copy-start(bf16[256,512]{1,0:T(8,128)(2,1)S(1)} %fusion.13.gated_ref) | copy-start | bytes 786436
  208.2 4.1 %collective-permute-start = (bf16[32,512]{1,0:T(8,128)(2,1)S(1)}, bf16[32,512]{1,0:T(8,128)(2,1)S(1)}, u32[]{:S(2)}, u32[]{:S(2)}) collective-permute-start(bf16[32,512]{1,0:T(8,128)(2,1)S(1)} %slice.77), channel_id=1, source_target_pairs={{0,8},{8,16},{16,24},{1,9},{9,17},{17,25},{2,10},{10,18},{18,26},{... | collective-permute-start | bytes 98312 | tf_op jit(solution)/shard_map/ppermute | solution.py:18
  212.3 0.6 copy-start.10
  225.2 5.6 %copy-start.4 = (bf16[256,512]{1,0:T(8,128)(2,1)S(1)}, bf16[256,512]{1,0:T(8,128)(2,1)}, u32[]{:S(2)}) copy-start(bf16[256,512]{1,0:T(8,128)(2,1)} %conv.1) | copy-start | bytes 786436
Sparse Core Ops, SparseCore 0:
  10.1 117.6 all-gather.4
  130.6 99.4 all-gather.2
  237.0 12.1 reduce-scatter.1
